TPU v7x, 32 devices: a whole 2x2x4 slice. The times are simulated.
32 devices in a mesh: ep: 8 (over z, x), tp: 4 (over y, core).
Axes of the slice: x: 2, y: 2, z: 4, core: 2. Of those that a mesh axis runs over, the one named last changes fastest.
Arguments:
- mixer_tokens: bfloat16 [1536, 2048], P('ep'), may hold values from -6 to 6
- mixer_gain: float32 [2048], replicated, may hold values from 0.1 to 1.9
- query_weight: bfloat16 [1024, 2048], P('tp'), may hold values from -1 to 1
- key_weight: bfloat16 [1024, 2048], P('tp'), may hold values from -1 to 1
- value_weight: bfloat16 [1024, 2048], P('tp'), may hold values from -0.125 to 0.125
- forget_weight: bfloat16 [2048, 16], P(None, 'tp'), may hold values from -0.125 to 0.125
- forget_bias: float32 [8, 16], P('ep', 'tp'), may hold values from 2.98 to 10.4
- output_weight: bfloat16 [1024, 2048], P(None, 'tp'), may hold values from -0.1875 to 0.1875
- expert_tokens: bfloat16 [1024, 2048], P('ep'), may hold values from -6 to 6
- expert_gain: float32 [2048], replicated, may hold values from 0.1 to 1.9
- routes: int32 [1024, 2], P('ep'), may hold values from 0 to 7, all different within a row; in each aligned block of 128 rows (0 to 127, 128 to 255, ...) at most 64 rows name the same one
- route_weights: float32 [1024, 2], P('ep'), may hold values from 0.2 to 1
- gate_weight: bfloat16 [8, 3584, 2048], P('ep', 'tp'), may hold values from -0.125 to 0.125
- up_weight: bfloat16 [8, 3584, 2048], P('ep', 'tp'), may hold values from -0.125 to 0.125
- down_weight: bfloat16 [8, 3584, 2048], P('ep', 'tp'), may hold values from -0.09375 to 0.09375
Outputs:
- mixer_output: bfloat16 [1536, 2048], P('ep', 'tp')
- expert_output: bfloat16 [1024, 2048], P('ep', 'tp')
Inputs may be any that keep to these rules, and one draw needn't show every extreme that they name: `routes`: within the tokens of one index of ep (aligned blocks of 128 rows) no expert is named more than 64 times, a bound that some block reaches; the 2 experts of a token differ.
All inputs are finite; a program needn't handle non-finite values.
Results may differ from a plain program's by a relative error of at most 0.019.
Values may be sent and summed in bfloat16 or wider, within the bound.
A program may use at most 128 MiB of HBM per device.

v0:
```python
import functools

import jax
import jax.numpy as jnp
from jax import lax
from jax.experimental import pallas as pl
from jax.experimental.pallas import tpu as pltpu
from jax.sharding import PartitionSpec as P

HD = 64
MEAN_FLOOR = 0.1
HEAD_FLOOR = 1.0
MESH = pl.DeviceIdType.MESH
VM = pl.BlockSpec(memory_space=pltpu.VMEM)
ANY = pl.BlockSpec(memory_space=pl.ANY)
DMA = pltpu.SemaphoreType.DMA
LIMIT = 48 << 20


def normed_rows(inputs, gain):
    values = inputs.astype(jnp.float32)
    square = jnp.mean(values * values, axis=-1, keepdims=True)
    return (values * lax.rsqrt(jnp.maximum(square, MEAN_FLOOR)) * gain).astype(jnp.bfloat16)


def by_rows(left, weight):
    return lax.dot_general(
        left, weight, (((1,), (1,)), ((), ())), preferred_element_type=jnp.float32
    )


class Place:
    def __init__(self, n_ep, n_tp):
        self.n_ep, self.n_tp, self.ny = n_ep, n_tp, n_tp // 2
        self.e = lax.axis_index("ep")
        self.t = lax.axis_index("tp")
        self.y, self.c = self.t // 2, self.t % 2
        self.partner = self.y * 2 + (1 - self.c)

    def ep(self, k):
        return (self.e + k) % self.n_ep

    def y_at(self, off):
        return (self.y + self.ny + off) % self.ny

    def chip(self, off):
        return self.y_at(off) * 2 + self.c

    def barrier(self):
        sem = pltpu.get_barrier_semaphore()
        for k in range(1, self.n_ep):
            pl.semaphore_signal(
                sem, inc=1, device_id={"ep": self.ep(k), "tp": self.t}, device_id_type=MESH
            )
        for off in range(1, self.ny):
            pl.semaphore_signal(
                sem, inc=1, device_id={"ep": self.e, "tp": self.chip(off)}, device_id_type=MESH
            )
        pl.semaphore_signal(
            sem, inc=1, device_id={"ep": self.e, "tp": self.partner}, device_id_type=MESH
        )
        pl.semaphore_wait(sem, self.n_ep - 1 + self.ny - 1 + 1)


def remote(src, dst, send, recv, e, t):
    return pltpu.make_async_remote_copy(
        src_ref=src,
        dst_ref=dst,
        send_sem=send,
        recv_sem=recv,
        device_id={"ep": e, "tp": t},
        device_id_type=MESH,
    )


class Exchange:
    def __init__(self, place, send, land, sems):
        self.p, self.send, self.land = place, send, land
        self.ssem, self.rsem = sems

    def copy(self, k):
        p = self.p
        d = p.ep(k)
        return remote(
            self.send(d), self.land(p.e), self.ssem.at[d], self.rsem.at[p.e], d, p.t
        )

    def arrival(self, k):
        p = self.p
        s = p.ep(k)
        return remote(self.send(s), self.land(s), self.ssem.at[s], self.rsem.at[s], s, p.t)

    def own(self):
        p = self.p
        return pltpu.make_async_copy(self.send(p.e), self.land(p.e), self.rsem.at[p.e])

    def start(self):
        for k in range(1, self.p.n_ep):
            self.copy(k).start()
        self.own().start()

    def wait_arrival(self, k):
        if k == 0:
            self.own().wait()
        else:
            self.arrival(k).wait_recv()

    def wait_sent(self):
        for k in range(1, self.p.n_ep):
            self.copy(k).wait_send()


class Spread:
    def __init__(self, place, land, sems):
        self.p, self.land = place, land
        self.ys, self.yr, self.ps, self.pr = sems

    def y_copy(self, off, s):
        p = self.p
        block = self.land(p.t, s)
        return remote(
            block, block, self.ys.at[off - 1, s], self.yr.at[off - 1, s], p.e, p.chip(off)
        )

    def y_arrival(self, off, s):
        p = self.p
        block = self.land(p.chip(-off), s)
        return remote(
            block, block, self.ys.at[off - 1, s], self.yr.at[off - 1, s], p.e, p.chip(-off)
        )

    def p_copy(self, off, s):
        p = self.p
        block = self.land(p.chip(-off), s)
        return remote(block, block, self.ps.at[off, s], self.pr.at[off, s], p.e, p.partner)

    def p_arrival(self, off, s):
        p = self.p
        block = self.land(p.y_at(-off) * 2 + (1 - p.c), s)
        return remote(block, block, self.ps.at[off, s], self.pr.at[off, s], p.e, p.partner)

    def first(self, s):
        for off in range(1, self.p.ny):
            self.y_copy(off, s).start()
        self.p_copy(0, s).start()

    def relay(self, s):
        for off in range(1, self.p.ny):
            self.y_arrival(off, s).wait_recv()
            self.p_copy(off, s).start()

    def finish(self, s):
        for off in range(self.p.ny):
            self.p_arrival(off, s).wait_recv()
        self.wait_sent(s)

    def wait_sent(self, s):
        for off in range(self.p.ny):
            self.p_copy(off, s).wait_send()
        for off in range(1, self.p.ny):
            self.y_copy(off, s).wait_send()


def spread_sems(n_ep, n_tp):
    ny = n_tp // 2
    far = max(ny - 1, 1)
    return [DMA((far, n_ep)), DMA((far, n_ep)), DMA((ny, n_ep)), DMA((ny, n_ep))]


def outward_kernel(
    n_ep, n_tp, slots, message, gates, gate_weight, up_weight,
    hidden, message_out, gates_out,
    out, gate_held, up_held, gate_act, up_act,
    s0, s1, m0, m1, g0, g1, w, ys, yr, ps, pr,
):
    p = Place(n_ep, n_tp)
    width = slots.shape[2]

    def cols(t):
        return pl.ds(pl.multiple_of(t * width, width), width)

    def land(t, s):
        return out.at[s, :, cols(t)]

    def multiply(t, opening):
        rows = out[:, :, cols(t)].reshape(hidden.shape[0], width)
        for held, total in ((gate_held, gate_act), (up_held, up_act)):
            product = by_rows(rows, held[:, cols(t)])
            total[...] = product if opening else total[...] + product

    loads = [
        pltpu.make_async_copy(gate_weight, gate_held, w.at[0]),
        pltpu.make_async_copy(up_weight, up_held, w.at[1]),
    ]
    for load in loads:
        load.start()
    p.barrier()
    slot_move = Exchange(p, lambda d: slots.at[d], lambda s: land(p.t, s), (s0, s1))
    gate_move = Exchange(p, lambda d: gates.at[d], lambda s: gates_out.at[s], (g0, g1))
    message_move = Exchange(p, lambda d: message.at[d], lambda s: message_out.at[s], (m0, m1))
    spread = Spread(p, land, (ys, yr, ps, pr))
    slot_move.start()
    gate_move.start()
    message_move.start()
    for k in range(n_ep):
        slot_move.wait_arrival(k)
        spread.first(p.ep(k))
    for load in loads:
        load.wait()
    multiply(p.t, True)
    for k in range(n_ep):
        spread.p_arrival(0, p.ep(k)).wait_recv()
    multiply(p.partner, False)
    for k in range(n_ep):
        spread.relay(p.ep(k))
    for off in range(1, p.ny):
        multiply(p.chip(-off), False)
        for k in range(n_ep):
            spread.p_arrival(off, p.ep(k)).wait_recv()
        multiply(p.y_at(-off) * 2 + (1 - p.c), False)
    gate = gate_act[...]
    hidden[...] = (gate * lax.logistic(gate) * up_act[...]).astype(hidden.dtype)
    for k in range(n_ep):
        gate_move.wait_arrival(k)
        message_move.wait_arrival(k)
        spread.wait_sent(p.ep(k))
    slot_move.wait_sent()
    gate_move.wait_sent()
    message_move.wait_sent()


def homeward_kernel(
    n_ep, n_tp, hidden, down_weight, heads, ret, heads_all,
    partial, down_held, pair, mine, out_y, in_y, final,
    w, h0, h1, a0, a1, r0, r1, q0, q1, ys, yr, ps, pr,
):
    p = Place(n_ep, n_tp)
    ny = p.ny
    width = ret.shape[2]

    def cols(t):
        return pl.ds(pl.multiple_of(t * width, width), width)

    def land(t, s):
        return heads_all.at[t, s]

    load = pltpu.make_async_copy(down_weight, down_held, w.at[0])
    load.start()
    p.barrier()
    head_move = Exchange(p, lambda d: heads.at[d], lambda s: land(p.t, s), (h0, h1))
    spread = Spread(p, land, (ys, yr, ps, pr))
    head_move.start()

    def pair_copy(s, off):
        src = partial.at[s, :, cols(p.y_at(off) * 2 + (1 - p.c))]
        return remote(src, pair.at[s, off], r0.at[s, off], r1.at[s, off], p.e, p.partner)

    def y_copy(s, off, to):
        return remote(
            out_y.at[s, off - 1], in_y.at[s, off - 1],
            q0.at[s, off - 1], q1.at[s, off - 1], p.e, p.chip(to),
        )

    def final_copy(k):
        d = p.ep(k)
        return remote(final.at[d], ret.at[p.e], a0.at[d], a1.at[p.e], d, p.t)

    order = list(range(1, n_ep)) + [0]
    capacity = ret.shape[1]

    def multiply(t):
        product = jnp.dot(
            hidden[...], down_held[:, cols(t)], preferred_element_type=jnp.float32
        )
        partial[:, :, cols(t)] = product.astype(jnp.bfloat16).reshape(n_ep, capacity, width)

    load.wait()
    turns = [*range(1, ny), 0]
    for off in turns:
        multiply(p.y_at(off) * 2 + (1 - p.c))
        multiply(p.chip(off))
        for k in order:
            pair_copy(p.ep(k), off).start()
        for k in order:
            s = p.ep(k)
            pair_copy(s, off).wait_recv()
            both = partial[s, :, cols(p.chip(off))].astype(jnp.float32) + pair[s, off].astype(
                jnp.float32
            )
            if off == 0:
                mine[s] = both
            else:
                out_y[s, off - 1] = both.astype(jnp.bfloat16)
                y_copy(s, off, off).start()
    for k in range(n_ep):
        head_move.wait_arrival(k)
        spread.first(p.ep(k))
    for k in order:
        s = p.ep(k)
        total = mine[s]
        for off in range(1, ny):
            y_copy(s, off, -off).wait_recv()
            total = total + in_y[s, off - 1].astype(jnp.float32)
        if k == 0:
            ret[s] = total.astype(jnp.bfloat16)
        else:
            final[s] = total.astype(jnp.bfloat16)
            final_copy(k).start()
    for k in range(n_ep):
        spread.relay(p.ep(k))
    for k in range(n_ep):
        spread.finish(p.ep(k))
    for k in range(n_ep):
        s = p.ep(k)
        for off in range(ny):
            pair_copy(s, off).wait_send()
        for off in range(1, ny):
            y_copy(s, off, off).wait_send()
    for k in range(1, n_ep):
        s = p.ep(k)
        remote(final.at[s], ret.at[s], a0.at[s], a1.at[s], s, p.t).wait_recv()
        final_copy(k).wait_send()
    head_move.wait_sent()


def outward(slots, message, gates, gate_weight, up_weight, n_ep, n_tp):
    _, capacity, width = slots.shape
    rows, units = n_ep * capacity, gate_weight.shape[0]
    scratch = [
        pltpu.VMEM((n_ep, capacity, width * n_tp), slots.dtype),
        pltpu.VMEM(gate_weight.shape, gate_weight.dtype),
        pltpu.VMEM(up_weight.shape, up_weight.dtype),
        pltpu.VMEM((rows, units), jnp.float32),
        pltpu.VMEM((rows, units), jnp.float32),
    ]
    sems = [DMA((n_ep,))] * 6 + [DMA((2,))] + spread_sems(n_ep, n_tp)
    return pl.pallas_call(
        functools.partial(outward_kernel, n_ep, n_tp),
        out_shape=[
            jax.ShapeDtypeStruct((rows, units), slots.dtype),
            jax.ShapeDtypeStruct(message.shape, message.dtype),
            jax.ShapeDtypeStruct(gates.shape, gates.dtype),
        ],
        in_specs=[VM] * 3 + [ANY] * 2,
        out_specs=[VM] * 3,
        scratch_shapes=scratch + sems,
        compiler_params=pltpu.CompilerParams(collective_id=0, has_side_effects=True),
        name="outward",
    )(slots, message, gates, gate_weight, up_weight)


def homeward(hidden, down_weight, heads, n_ep, n_tp):
    capacity, features = hidden.shape[0] // n_ep, down_weight.shape[1]
    width, ny = features // n_tp, n_tp // 2
    far = max(ny - 1, 1)
    scratch = [
        pltpu.VMEM((n_ep, capacity, features), jnp.bfloat16),
        pltpu.VMEM(down_weight.shape, down_weight.dtype),
        pltpu.VMEM((n_ep, ny, capacity, width), jnp.bfloat16),
        pltpu.VMEM((n_ep, capacity, width), jnp.float32),
        pltpu.VMEM((n_ep, far, capacity, width), jnp.bfloat16),
        pltpu.VMEM((n_ep, far, capacity, width), jnp.bfloat16),
        pltpu.VMEM((n_ep, capacity, width), jnp.bfloat16),
    ]
    sems = [DMA((1,))] + [DMA((n_ep,))] * 4 + [DMA((n_ep, ny))] * 2 + [DMA((n_ep, far))] * 2
    return pl.pallas_call(
        functools.partial(homeward_kernel, n_ep, n_tp),
        out_shape=[
            jax.ShapeDtypeStruct((n_ep, capacity, width), jnp.bfloat16),
            jax.ShapeDtypeStruct((n_tp,) + heads.shape, jnp.bfloat16),
        ],
        in_specs=[VM, ANY, VM],
        out_specs=[VM] * 2,
        scratch_shapes=scratch + sems + spread_sems(n_ep, n_tp),
        compiler_params=pltpu.CompilerParams(collective_id=1, has_side_effects=True),
        name="homeward",
    )(hidden, down_weight, heads)


def on_device(
    mixer_tokens,
    mixer_gain,
    query_weight,
    key_weight,
    value_weight,
    forget_weight,
    forget_bias,
    output_weight,
    expert_tokens,
    expert_gain,
    routes,
    route_weights,
    gate_weight,
    up_weight,
    down_weight,
):
    n_ep, n_tp = lax.axis_size("ep"), lax.axis_size("tp")
    rows, features = mixer_tokens.shape
    local_heads = forget_weight.shape[1]
    share = n_ep // local_heads
    part = rows // share
    width = features // n_tp
    bf16, f32 = jnp.bfloat16, jnp.float32

    expert_normed = normed_rows(expert_tokens, expert_gain)
    token_count, top_count = routes.shape
    capacity = 2 * top_count * token_count // n_ep
    pairs = token_count * top_count
    flat_routes = routes.reshape(-1)
    onehot = flat_routes[:, None] == jnp.arange(n_ep, dtype=jnp.int32)[None, :]
    before = jnp.tril(jnp.ones((pairs, pairs), bf16), -1)
    ranks = jnp.dot(before, onehot.astype(bf16), preferred_element_type=f32)
    slot_rank = jnp.sum(jnp.where(onehot, ranks, 0.0), axis=1).astype(jnp.int32)
    slot_index = (flat_routes * capacity + slot_rank).reshape(token_count, top_count)
    slot_ids = jnp.arange(n_ep * capacity, dtype=jnp.int32)
    picks = [(slot_index[:, j][:, None] == slot_ids[None, :]).astype(bf16) for j in range(top_count)]
    column = lax.axis_index("tp") * width
    own_columns = lax.dynamic_slice_in_dim(expert_normed, column, width, 1)
    slots = lax.dot_general(
        sum(picks[1:], picks[0]), own_columns, (((0,), (0,)), ((), ())),
        preferred_element_type=f32,
    ).astype(bf16).reshape(n_ep, capacity, width)

    normed = normed_rows(mixer_tokens, mixer_gain)
    queries = by_rows(normed, query_weight).astype(bf16)
    key_rows = by_rows(normed, key_weight).astype(bf16)
    value_rows = by_rows(normed, value_weight).astype(bf16)
    pre_gate = jnp.dot(normed, forget_weight, preferred_element_type=f32) + forget_bias
    block_cum = jnp.dot(
        jnp.tril(jnp.ones((rows, rows), f32)), jax.nn.log_sigmoid(pre_gate),
        precision=lax.Precision.HIGHEST, preferred_element_type=f32,
    )
    key_value = jnp.concatenate(
        [
            key_rows.reshape(rows, local_heads, HD).transpose(1, 0, 2),
            value_rows.reshape(rows, local_heads, HD).transpose(1, 0, 2),
        ],
        axis=2,
    )
    key_value = jnp.broadcast_to(
        key_value[:, None], (local_heads, share, rows, 2 * HD)
    ).reshape(n_ep, rows, 2 * HD)
    half = part // 2
    query_parts = queries.reshape(share, 2, half, local_heads, HD).transpose(3, 0, 2, 1, 4)
    query_parts = query_parts.reshape(n_ep, half, 2 * HD)
    message = jnp.concatenate([key_value, query_parts], axis=1)
    gates = jnp.broadcast_to(block_cum.T[:, None, None, :], (local_heads, share, 1, rows))
    gates = gates.reshape(n_ep, 1, rows)

    hidden, all_messages, all_gates = outward(
        slots, message, gates, gate_weight[0], up_weight[0], n_ep, n_tp
    )

    positions = n_ep * rows
    all_gates = all_gates.reshape(n_ep, rows)
    totals = all_gates[:, rows - 1]
    lower = jnp.arange(n_ep)[None, :] < jnp.arange(n_ep)[:, None]
    base = jnp.sum(jnp.where(lower, totals[None, :], 0.0), axis=1)
    cumulative = all_gates + base[:, None]
    keys = all_messages[:, :rows, :HD].reshape(positions, HD)
    values = all_messages[:, :rows, HD:].reshape(positions, HD)
    head_query = all_messages[:, rows:].reshape(n_ep, half, 2, HD).transpose(0, 2, 1, 3)
    head_query = head_query.reshape(n_ep * part, HD)
    first = (lax.axis_index("ep") % share) * part
    query_cum = lax.dynamic_slice_in_dim(cumulative, first, part, 1).reshape(-1)
    query_pos = (
        jnp.arange(n_ep, dtype=jnp.int32)[:, None] * rows
        + first
        + jnp.arange(part, dtype=jnp.int32)[None, :]
    ).reshape(-1)
    key_pos = jnp.arange(positions, dtype=jnp.int32)
    scores = by_rows(head_query, keys) * HD ** (-0.5)
    scores = scores + query_cum[:, None] - cumulative.reshape(-1)[None, :]
    scores = jnp.where(key_pos[None, :] <= query_pos[:, None], scores, -jnp.inf)
    weights = jnp.exp(scores - jnp.max(scores, axis=-1, keepdims=True)).astype(bf16)
    attended = jnp.dot(weights, values, preferred_element_type=f32)
    rescale = lax.rsqrt(jnp.mean(attended * attended, axis=-1, keepdims=True) + HEAD_FLOOR)
    head_out = (attended * rescale).astype(bf16).reshape(n_ep, part, HD)

    returned, heads_all = homeward(hidden, down_weight[0], head_out, n_ep, n_tp)

    heads_all = heads_all.reshape(n_tp, local_heads, share, part, HD).transpose(2, 3, 0, 1, 4)
    heads_all = heads_all.reshape(rows, n_tp * local_heads * HD)
    mixer_output = jnp.dot(heads_all, output_weight, preferred_element_type=f32).astype(bf16)
    returned = returned.reshape(n_ep * capacity, width)
    expert_output = 0.0
    for j in range(top_count):
        picked = jnp.dot(picks[j], returned, preferred_element_type=f32)
        expert_output = expert_output + picked * route_weights[:, j][:, None]
    return (mixer_output, expert_output.astype(bf16))


def lanes_of(shape, dim):
    return lax.broadcasted_iota(jnp.int32, shape, dim)


def flipped(place, bits):
    at, weight = place, 1
    while bits:
        if bits % 2:
            at = at + weight * (1 - 2 * (place // weight % 2))
        bits, weight = bits // 2, weight * 2
    return at


def fused_kernel(
    n_ep, n_tp,
    tokens_a, gain_a, w_q, w_k, w_v, w_f, b_f, w_o, tokens_b, gain_b, routes, route_w,
    w_gate, w_up, w_down,
    out_a, out_b,
    a_held, ga_held, q_held, kv_held, f_held, bf_held, o_held, b_held, gb_held, r_held, rw_held,
    gate_held, up_held, down_held,
    slots, land, w_hi, w_lo, kv_send, q_send, g_send, kv_land, q_land, g_land,
    hidden, pair_send, pair_land, own_part, mine, y_send, y_land, final, ret,
    q_all, q_cum, scores, running, row_max, attended, head_send, heads_all, lhs,
    lsem, s0, s1, ys, yr, ps, pr, k0, k1, x0, x1, q0, q1, g0, g1,
    p0, p1, z0, z1, a0, a1, h0, h1, hy0, hy1, hp0, hp1,
):
    p = Place(n_ep, n_tp)
    ny = p.ny
    bf16, f32 = jnp.bfloat16, jnp.float32
    rows, features = a_held.shape
    tokens = b_held.shape[0]
    _, capacity, width = slots.shape
    local_heads = kv_send.shape[0]
    share = n_ep // local_heads
    part = rows // share
    half = part // 2
    units = gate_held.shape[0]
    near, quarter = range(n_ep // 2), n_ep // 4
    third, second = range(n_ep // 2, 3 * quarter), range(3 * quarter, n_ep)
    groups = [near, second, third]
    own_share = p.e % share
    first = own_share * part

    def cols(t):
        return pl.ds(pl.multiple_of(t * width, width), width)

    def peer(j):
        return flipped(p.e, j)

    barrier = pltpu.get_barrier_semaphore()
    for k in range(1, n_ep):
        pl.semaphore_signal(
            barrier, inc=1, device_id={"ep": p.ep(k), "tp": p.t}, device_id_type=MESH
        )
    for off in range(1, ny):
        pl.semaphore_signal(
            barrier, inc=1, device_id={"ep": p.e, "tp": p.chip(off)}, device_id_type=MESH
        )
    pl.semaphore_signal(
        barrier, inc=1, device_id={"ep": p.e, "tp": p.partner}, device_id_type=MESH
    )

    early = [(tokens_b, b_held), (routes, r_held), (gain_b, gb_held)]
    middle = [(tokens_a, a_held), (gain_a, ga_held), (w_f, f_held), (b_f, bf_held)]
    for h in range(local_heads):
        mine_rows = pl.ds(h * HD, HD)
        middle.append((w_k.at[mine_rows], kv_held.at[pl.ds(2 * h * HD, HD)]))
        middle.append((w_v.at[mine_rows], kv_held.at[pl.ds((2 * h + 1) * HD, HD)]))
    middle.append((w_q, q_held))
    late = [
        (w_gate, gate_held), (w_up, up_held), (w_down, down_held), (route_w, rw_held),
        (w_o, o_held),
    ]
    loads, number = [], 0
    for batch in (early, middle, late):
        made = []
        for src, dst in batch:
            made.append(pltpu.make_async_copy(src, dst, lsem.at[number]))
            number += 1
        loads.append(made)
    early, middle, late = loads
    for load in early + middle:
        load.start()

    for load in early:
        load.wait()
    values = b_held[...].astype(f32)
    square = jnp.mean(values * values, axis=-1, keepdims=True)
    scale = lax.rsqrt(jnp.maximum(square, MEAN_FLOOR))
    own_columns = (b_held[:, cols(p.t)].astype(f32) * scale * gb_held[:, cols(p.t)]).astype(bf16)
    named_by = r_held[...]
    top_count = named_by.shape[0]
    place = lanes_of((n_ep, tokens), 0)
    expert_at, weight = place, 1
    while weight < n_ep:
        flip = (p.e // weight) % 2
        expert_at = expert_at + flip * weight * (1 - 2 * ((place // weight) % 2))
        weight *= 2
    chosen = [named_by[c : c + 1, :] == expert_at for c in range(top_count)]
    named = sum([c.astype(f32) for c in chosen[1:]], chosen[0].astype(f32))
    earlier = (lanes_of((tokens, tokens), 0) < lanes_of((tokens, tokens), 1)).astype(bf16)
    ranks = jnp.dot(named.astype(bf16), earlier, preferred_element_type=f32)
    ranks = jnp.where(named > 0, ranks, -1.0).astype(jnp.int32)
    slot_at = lanes_of((capacity, tokens), 0)
    picks = [ranks[j : j + 1, :] == slot_at for j in range(n_ep)]
    for j in range(n_ep):
        block = jnp.dot(
            picks[j].astype(f32).astype(bf16), own_columns, preferred_element_type=f32
        ).astype(bf16)
        if j == 0:
            land[0, :, cols(p.t)] = block
        else:
            slots[j] = block
    pl.semaphore_wait(barrier, n_ep - 1 + ny - 1 + 1)

    def slot_copy(j):
        return remote(
            slots.at[j], land.at[j, :, cols(p.t)], s0.at[j], s1.at[j], peer(j), p.t
        )

    spread = Spread(p, lambda t, j: land.at[j, :, cols(t)], (ys, yr, ps, pr))
    for j in [*near[1:], *second, *third]:
        slot_copy(j).start()
    spread.first(0)

    for load in middle:
        load.wait()
    for load in late:
        load.start()
    values = a_held[...].astype(f32)
    square = jnp.mean(values * values, axis=-1, keepdims=True)
    scale = lax.rsqrt(jnp.maximum(square, MEAN_FLOOR))
    a_held[...] = (values * scale * ga_held[...]).astype(bf16)
    normed = a_held[...]
    eye = lanes_of((local_heads, local_heads), 0) == lanes_of((local_heads, local_heads), 1)
    bias = jnp.sum(jnp.where(eye, bf_held[...], 0.0), axis=1, keepdims=True)
    gate = by_rows(f_held[...], normed) + bias
    log_gate = jnp.minimum(gate, 0.0) - jnp.log1p(jnp.exp(-jnp.abs(gate)))
    upto = (lanes_of((rows, rows), 0) <= lanes_of((rows, rows), 1)).astype(f32)
    block_cum = jnp.dot(
        log_gate, upto, precision=lax.Precision.HIGHEST, preferred_element_type=f32
    )
    for h in range(local_heads):
        g_send[h] = block_cum[h : h + 1, :]

    def kv_copy(h):
        to = h * share + own_share
        return remote(kv_send.at[h], kv_land.at[p.e], k0.at[h], k1.at[p.e], to, p.t)

    def kv_arrival(n):
        s = (p.e // share + n) % local_heads * share + own_share
        return remote(kv_send.at[0], kv_land.at[s], k0.at[0], k1.at[s], p.e, p.t), s

    def sibling(off):
        return p.e // share * share + (own_share + off) % share

    def kv_relay(s, off):
        return remote(
            kv_land.at[s], kv_land.at[s], x0.at[off, s], x1.at[s], sibling(off), p.t
        )

    def q_copy(k):
        d = p.ep(k)
        return remote(q_send.at[d], q_land.at[p.e], q0.at[d], q1.at[p.e], d, p.t)

    def q_arrival(k):
        s = p.ep(k)
        return remote(q_send.at[s], q_land.at[s], q0.at[s], q1.at[s], s, p.t)

    def g_copy(k):
        d = p.ep(k)
        return remote(g_send.at[d // share], g_land.at[p.e], g0.at[d], g1.at[p.e], d, p.t)

    def g_arrival(k):
        s = p.ep(k)
        return remote(g_send.at[0], g_land.at[s], g0.at[s], g1.at[s], s, p.t)

    key_value = by_rows(normed, kv_held[...]).astype(bf16)
    for h in range(local_heads):
        kv_send[h] = key_value[:, 2 * h * HD : 2 * (h + 1) * HD]
    for n in range(1, local_heads):
        kv_copy((p.e // share + n) % local_heads).start()
    own_head = p.e // share
    kv_land[p.e] = kv_send[own_head]
    for off in range(1, share):
        kv_relay(p.e, off).start()
    slot_copy(1).wait_recv()
    spread.first(1)
    queries = by_rows(normed, q_held[...]) * HD ** (-0.5)
    left = lanes_of((half, 2 * HD), 1) < HD
    for pair in range(local_heads // 2):
        there = queries[:, 2 * pair * HD : 2 * (pair + 1) * HD]
        moved = pltpu.roll(there, HD, 1)
        for x in range(share):
            top, bottom = slice(x * part, x * part + half), slice(x * part + half, (x + 1) * part)
            q_send[2 * pair * share + x] = jnp.where(left, there[top], moved[bottom]).astype(bf16)
            q_send[(2 * pair + 1) * share + x] = jnp.where(
                left, moved[top], there[bottom]
            ).astype(bf16)
    for k in range(1, n_ep):
        q_copy(k).start()
        g_copy(k).start()
    q_land[p.e] = q_send[p.e]
    g_land[p.e] = g_send[own_head]

    def arrive(j):
        slot_copy(j).wait_recv()
        spread.first(j)

    def complete(j):
        spread.relay(j)

    def settle(j):
        for off in range(ny):
            spread.p_arrival(off, j).wait_recv()

    cuts = [(at, min(at + 256, units)) for at in range(0, units, 256)]

    def open_up(g, beside):
        low_row, count = groups[g][0], len(groups[g])
        block = land[low_row : low_row + count].reshape(count * capacity, features)
        lines = slice(low_row * capacity, (low_row + count) * capacity)
        for number, (low, high) in enumerate(cuts):
            gated = by_rows(block, gate_held[low:high])
            upped = by_rows(block, up_held[low:high])
            hidden[lines, low:high] = (gated * lax.logistic(gated) * upped).astype(bf16)
            for act in beside[number : number + 1]:
                act()
        for act in beside[len(cuts) :]:
            act()

    def pair_copy(g, off):
        low_row, count = groups[g][0], len(groups[g])
        lines = pl.ds(low_row * capacity, count * capacity)
        return remote(
            pair_send.at[off, lines], pair_land.at[off, lines], p0.at[g, off], p1.at[g, off],
            p.e, p.partner,
        )

    def y_copy(j, off, to):
        return remote(
            y_send.at[j, off - 1], y_land.at[j, off - 1],
            z0.at[j, off - 1], z1.at[j, off - 1], p.e, p.chip(to),
        )

    turns = [*range(1, ny), 0]

    def close_down(g):
        low_row, count = groups[g][0], len(groups[g])
        lines = slice(low_row * capacity, (low_row + count) * capacity)

        def product(t):
            return jnp.dot(hidden[lines], down_held[:, cols(t)], preferred_element_type=f32)

        for off in turns:
            pair_send[off, lines] = product(p.y_at(off) * 2 + (1 - p.c)).astype(bf16)
            pair_copy(g, off).start()
        for off in turns:
            own_part[lines] = product(p.chip(off))
            pair_copy(g, off).wait_recv()
            both = own_part[lines] + pair_land[off, lines].astype(f32)
            both = both.reshape(count, capacity, width)
            for m in range(count):
                j = low_row + m
                if off == 0:
                    mine[j] = both[m]
                else:
                    y_send[j, off - 1] = both[m].astype(bf16)
                    y_copy(j, off, off).start()

    def final_copy(j):
        return remote(final.at[j], ret.at[j], a0.at[j], a1.at[j], peer(j), p.t)

    def finish(j):
        total = mine[j]
        for off in range(1, ny):
            y_copy(j, off, -off).wait_recv()
            total = total + y_land[j, off - 1].astype(f32)
        if j == 0:
            ret[0] = total.astype(bf16)
        else:
            final[j] = total.astype(bf16)
            final_copy(j).start()

    def kv_forward(n):
        copy, s = kv_arrival(n)
        copy.wait_recv()
        for off in range(1, share):
            kv_relay(s, off).start()

    for j in near[2:]:
        arrive(j)
    for j in near:
        complete(j)
    for j in near:
        settle(j)
    late[0].wait()
    late[1].wait()
    open_up(0, [functools.partial(arrive, j) for j in second])
    for j in second:
        complete(j)
    for j in second:
        settle(j)
    open_up(1, [])
    late[2].wait()
    close_down(1)
    for j in third:
        arrive(j)
    close_down(0)
    for j in third:
        complete(j)
    for j in second:
        finish(j)
    for j in third:
        settle(j)
    open_up(2, [functools.partial(kv_forward, n) for n in range(1, local_heads)])
    close_down(2)
    for j in near:
        finish(j)

    late[3].wait()
    for j in range(n_ep):
        weight = 0.0
        for c in range(top_count):
            weight = weight + jnp.where(
                named_by[c : c + 1, :] == peer(j), rw_held[c : c + 1, :], 0.0
            )
        weight = jnp.where(ranks[j : j + 1, :] == slot_at, weight, 0.0)
        high = weight.astype(bf16)
        w_hi[j * capacity : (j + 1) * capacity] = high
        w_lo[j * capacity : (j + 1) * capacity] = (weight - high.astype(f32)).astype(bf16)

    for k in range(1, n_ep):
        g_arrival(k).wait_recv()
        q_arrival(k).wait_recv()
    for off in range(1, share):
        for n in range(local_heads):
            s = (p.e // share + n) % local_heads * share + (own_share + share - off) % share
            remote(kv_send.at[0], kv_land.at[s], k0.at[0], x1.at[s], p.e, p.t).wait_recv()
    positions = lanes_of((part, rows), 1)
    asked = first + lanes_of((part, rows), 0)
    base = jnp.zeros((1, 1), f32)
    key_cum = []
    last = lanes_of((1, rows), 1) == rows - 1
    for b in range(n_ep):
        block = g_land[b]
        key_cum.append(block + base)
        base = base + jnp.sum(jnp.where(last, block, 0.0), axis=1, keepdims=True)
        at = b * part
        q_cum[at : at + part] = jnp.sum(
            jnp.where(positions == asked, key_cum[b], 0.0), axis=1, keepdims=True
        )
        packed = q_land[b].astype(f32)
        q_all[at : at + half] = jnp.where(left, packed, 0.0).astype(bf16)
        q_all[at + half : at + part] = jnp.where(
            left, pltpu.roll(packed, HD, 1), 0.0
        ).astype(bf16)
    for b in range(n_ep):
        at = b * part
        block = by_rows(q_all[at:], kv_land[b]) + q_cum[at:] - key_cum[b]
        seen = jnp.where(positions <= asked, block[:part], -jnp.inf)
        scores[b, at : at + part] = seen
        if b == 0:
            running[:part] = seen
            running[part:] = block[part:]
        else:
            running[at : at + part] = jnp.maximum(running[at : at + part], seen)
        if b + 1 < n_ep:
            scores[b, at + part :] = block[part:]
            if b > 0:
                running[at + part :] = jnp.maximum(running[at + part :], block[part:])
    row_max[...] = jnp.max(running[...], axis=1, keepdims=True)
    for b in range(n_ep):
        at = b * part
        weights = jnp.exp(scores[b, at:] - row_max[at:]).astype(bf16)
        product = jnp.dot(weights, kv_land[b], preferred_element_type=f32)
        if b == 0:
            attended[...] = product
        else:
            attended[at:] = attended[at:] + product
    right = lanes_of((part, 2 * HD), 1) >= HD
    for b in range(n_ep):
        block = jnp.where(right, attended[b * part : (b + 1) * part], 0.0)
        block = block * lax.rsqrt(
            jnp.sum(block * block, axis=1, keepdims=True) * (1.0 / HD) + HEAD_FLOOR
        )
        moved = pltpu.roll(block, HD, 1)
        head_send[b] = jnp.where(left, moved[:half], block[half:]).astype(bf16)

    def head_copy(k):
        d = peer(k)
        return remote(head_send.at[d], heads_all.at[p.t, p.e], h0.at[d], h1.at[p.e], d, p.t)

    def head_arrival(k):
        s = peer(k)
        return remote(head_send.at[s], heads_all.at[p.t, s], h0.at[s], h1.at[s], s, p.t)

    for k in range(1, n_ep):
        head_copy(k).start()
    heads_all[p.t, p.e] = head_send[p.e]

    for j in third:
        finish(j)

    gather = Spread(p, lambda t, s: heads_all.at[t, s], (hy0, hy1, hp0, hp1))
    gather.first(p.e)
    for k in range(1, n_ep):
        head_arrival(k).wait_recv()
        gather.first(peer(k))
    for k in range(n_ep):
        gather.relay(peer(k))
    for k in range(n_ep):
        for off in range(ny):
            gather.p_arrival(off, peer(k)).wait_recv()
    for t in range(n_tp):
        for pair in range(local_heads // 2):
            lanes = slice((t * local_heads + 2 * pair) * HD, (t * local_heads + 2 * pair + 2) * HD)
            for x in range(share):
                one = heads_all[t, 2 * pair * share + x].astype(f32)
                two = heads_all[t, (2 * pair + 1) * share + x].astype(f32)
                at = x * part
                lhs[at : at + half, lanes] = jnp.where(
                    left, one, pltpu.roll(two, HD, 1)
                ).astype(bf16)
                lhs[at + half : at + part, lanes] = jnp.where(
                    left, pltpu.roll(one, HD, 1), two
                ).astype(bf16)
    late[4].wait()
    out_a[...] = jnp.dot(lhs[...], o_held[...], preferred_element_type=f32).astype(bf16)

    for j in range(1, n_ep):
        final_copy(j).wait_recv()
    returned = ret[...].reshape(n_ep * capacity, width)
    over_slots = (((0,), (0,)), ((), ()))
    total = lax.dot_general(w_hi[...], returned, over_slots, preferred_element_type=f32)
    total = total + lax.dot_general(w_lo[...], returned, over_slots, preferred_element_type=f32)
    out_b[...] = total.astype(bf16)

    for j in range(n_ep):
        spread.wait_sent(j)
        gather.wait_sent(peer(j))
        for off in range(1, ny):
            y_copy(j, off, off).wait_send()
    for j in range(1, n_ep):
        slot_copy(j).wait_send()
        final_copy(j).wait_send()
        q_copy(j).wait_send()
        g_copy(j).wait_send()
        head_copy(j).wait_send()
    for n in range(1, local_heads):
        kv_copy((p.e // share + n) % local_heads).wait_send()
    for n in range(local_heads):
        s = (p.e // share + n) % local_heads * share + own_share
        for off in range(1, share):
            kv_relay(s, off).wait_send()
    for g in range(len(groups)):
        for off in range(ny):
            pair_copy(g, off).wait_send()


def fused_on_device(
    mixer_tokens, mixer_gain, query_weight, key_weight, value_weight, forget_weight,
    forget_bias, output_weight, expert_tokens, expert_gain, routes, route_weights,
    gate_weight, up_weight, down_weight,
):
    n_ep, n_tp = lax.axis_size("ep"), lax.axis_size("tp")
    ny = n_tp // 2
    far = max(ny - 1, 1)
    rows, features = mixer_tokens.shape
    tokens, top_count = routes.shape
    local_heads = forget_weight.shape[1]
    share = n_ep // local_heads
    part = rows // share
    half = part // 2
    width = features // n_tp
    capacity = 2 * top_count * tokens // n_ep
    units = gate_weight.shape[1]
    groups = 3
    asked = n_ep * part
    bf16, f32 = jnp.bfloat16, jnp.float32
    operands = [
        mixer_tokens, mixer_gain.reshape(1, features), query_weight, key_weight, value_weight,
        forget_weight.T, forget_bias, output_weight, expert_tokens,
        expert_gain.reshape(1, features), routes.T, route_weights.T,
        gate_weight[0], up_weight[0], down_weight[0],
    ]
    operands = [pltpu.with_memory_space_constraint(x, pltpu.HBM) for x in operands]
    vmem = pltpu.VMEM
    scratch = [
        vmem((rows, features), bf16), vmem((1, features), f32),
        vmem(query_weight.shape, bf16), vmem((2 * local_heads * HD, features), bf16),
        vmem((local_heads, features), bf16), vmem((1, local_heads), f32),
        vmem(output_weight.shape, bf16), vmem((tokens, features), bf16),
        vmem((1, features), f32), vmem((top_count, tokens), jnp.int32),
        vmem((top_count, tokens), f32),
        vmem((units, features), bf16), vmem((units, features), bf16),
        vmem((units, features), bf16),
        vmem((n_ep, capacity, width), bf16), vmem((n_ep, capacity, features), bf16),
        vmem((n_ep * capacity, tokens), bf16), vmem((n_ep * capacity, tokens), bf16),
        vmem((local_heads, rows, 2 * HD), bf16), vmem((n_ep, half, 2 * HD), bf16),
        vmem((local_heads, 1, rows), f32),
        vmem((n_ep, rows, 2 * HD), bf16), vmem((n_ep, half, 2 * HD), bf16),
        vmem((n_ep, 1, rows), f32),
        vmem((n_ep * capacity, units), bf16),
        vmem((ny, n_ep * capacity, width), bf16),
        vmem((ny, n_ep * capacity, width), bf16),
        vmem((n_ep * capacity, width), f32),
        vmem((n_ep, capacity, width), f32),
        vmem((n_ep, far, capacity, width), bf16), vmem((n_ep, far, capacity, width), bf16),
        vmem((n_ep, capacity, width), bf16), vmem((n_ep, capacity, width), bf16),
        vmem((asked, 2 * HD), bf16), vmem((asked, 1), f32),
        vmem((n_ep, asked, rows), f32), vmem((asked, rows), f32), vmem((asked, 1), f32),
        vmem((asked, 2 * HD), f32), vmem((n_ep, half, 2 * HD), bf16),
        vmem((n_tp, n_ep, half, 2 * HD), bf16), vmem((rows, n_tp * local_heads * HD), bf16),
    ]
    sems = [DMA((13 + 2 * local_heads,)), DMA((n_ep,)), DMA((n_ep,))] + spread_sems(n_ep, n_tp)
    sems += [DMA((local_heads,)), DMA((n_ep,)), DMA((share, n_ep)), DMA((n_ep,))]
    sems += [DMA((n_ep,))] * 4 + [DMA((groups, ny))] * 2 + [DMA((n_ep, far))] * 2
    sems += [DMA((n_ep,))] * 4 + spread_sems(n_ep, n_tp)
    return pl.pallas_call(
        functools.partial(fused_kernel, n_ep, n_tp),
        out_shape=[
            jax.ShapeDtypeStruct((rows, width), bf16),
            jax.ShapeDtypeStruct((tokens, width), bf16),
        ],
        in_specs=[ANY] * len(operands),
        out_specs=[VM] * 2,
        scratch_shapes=scratch + sems,
        compiler_params=pltpu.CompilerParams(
            collective_id=2, has_side_effects=True, vmem_limit_bytes=LIMIT
        ),
        name="fused",
    )(*operands)


def deliver_kernel(one, two, one_out, two_out, sem):
    copies = [
        pltpu.make_async_copy(one, one_out, sem.at[0]),
        pltpu.make_async_copy(two, two_out, sem.at[1]),
    ]
    for copy in copies:
        copy.start()
    for copy in copies:
        copy.wait()


def deliver(one, two):
    return pl.pallas_call(
        deliver_kernel,
        out_shape=[
            jax.ShapeDtypeStruct(one.shape, one.dtype),
            jax.ShapeDtypeStruct(two.shape, two.dtype),
        ],
        in_specs=[ANY] * 2,
        out_specs=[ANY] * 2,
        scratch_shapes=[DMA((2,))],
        compiler_params=pltpu.CompilerParams(vmem_limit_bytes=1 << 20),
        name="deliver",
    )(one, two)


def choose(*arguments):
    n_ep = lax.axis_size("ep")
    rows, local_heads = arguments[0].shape[0], arguments[5].shape[1]
    share = n_ep // local_heads
    packed = local_heads % 2 == 0 and n_ep % local_heads == 0
    packed = packed and n_ep >= 8 and n_ep & (n_ep - 1) == 0
    if packed and rows % (32 * share) == 0:
        return tuple(deliver(*fused_on_device(*arguments)))
    return on_device(*arguments)


def solution(mesh):
    in_specs = (
        P("ep", None),
        P(),
        P("tp", None),
        P("tp", None),
        P("tp", None),
        P(None, "tp"),
        P("ep", "tp"),
        P(None, "tp"),
        P("ep", None),
        P(),
        P("ep", None),
        P("ep", None),
        P("ep", "tp", None),
        P("ep", "tp", None),
        P("ep", "tp", None),
    )
    out_specs = (P("ep", "tp"), P("ep", "tp"))
    return jax.shard_map(
        choose, mesh=mesh, in_specs=in_specs, out_specs=out_specs, check_vma=False
    )
```

profile of v0, /device:TPU:0, one launch (start us, length us, event | category | flops | bytes accessed | tf_op | source)
XLA Modules:
  0.0 60.2 jit_solution(7508324781792963365)
XLA Ops:
  0.6 58.8 %fused.1 = (bf16[192,512]{1,0:T(8,128)(2,1)S(1)}, bf16[128,512]{1,0:T(8,128)(2,1)S(1)}) custom-call(bf16[192,2048]{1,0:T(8,128)(2,1)} %tokens_a.1, f32[1,2048]{1,0:T(1,128)} %bitcast.12, bf16[256,2048]{1,0:T(8,128)(2,1)} %w_q.1, bf16[256,2048]{1,0:T(8,128)(2,1)} %w_k.1, bf16[256,2048]{1,0:T(8,128)(2,1)} %w_v.1, bf16[4,2048]{1,0:T(4,128)(2,1)} %bitcast.11, ...), custom_call_target="tpu_custom_call" | custom-call | tf_op jit(solution)/shard_map/fused/pallas_call | solution.py:1012
  59.4 0.7 %deliver.1 = (bf16[192,512]{1,0:T(8,128)(2,1)}, bf16[128,512]{1,0:T(8,128)(2,1)}) custom-call(bf16[192,512]{1,0:T(8,128)(2,1)S(1)} %get-tuple-element.4.one, bf16[128,512]{1,0:T(8,128)(2,1)S(1)} %get-tuple-element.5.two), custom_call_target="tpu_custom_call" | custom-call | tf_op jit(solution)/shard_map/deliver/pallas_call | solution.py:1040
where the time goes:
time: 61 us; the launch traced here: 60.2 us
  Pallas kernels  59.5 us (98%)
  between operations  0.64 us (1%)
    pallas_call x1, Pallas kernels, fused_on_device(): pl.pallas_call(functools.partial(fused_kernel, n_ep, n_tp), out_shape=[ja...  58.8 us

commit v1 on v0

--- a/solution.py
+++ b/solution.py
@@ -708,6 +708,10 @@
 
     cuts = [(at, min(at + 256, units)) for at in range(0, units, 256)]
 
+    def serve(beside, number, count):
+        for act, *given in beside[len(beside) * number // count : len(beside) * (number + 1) // count]:
+            act(*given)
+
     def open_up(g, beside):
         low_row, count = groups[g][0], len(groups[g])
         block = land[low_row : low_row + count].reshape(count * capacity, features)
@@ -716,10 +720,7 @@
             gated = by_rows(block, gate_held[low:high])
             upped = by_rows(block, up_held[low:high])
             hidden[lines, low:high] = (gated * lax.logistic(gated) * upped).astype(bf16)
-            for act in beside[number : number + 1]:
-                act()
-        for act in beside[len(cuts) :]:
-            act()
+            serve(beside, number, len(cuts))
 
     def pair_copy(g, off):
         low_row, count = groups[g][0], len(groups[g])
@@ -737,18 +738,20 @@
 
     turns = [*range(1, ny), 0]
 
-    def close_down(g):
+    def close_down(g, beside):
         low_row, count = groups[g][0], len(groups[g])
         lines = slice(low_row * capacity, (low_row + count) * capacity)
 
         def product(t):
             return jnp.dot(hidden[lines], down_held[:, cols(t)], preferred_element_type=f32)
 
-        for off in turns:
+        for number, off in enumerate(turns):
             pair_send[off, lines] = product(p.y_at(off) * 2 + (1 - p.c)).astype(bf16)
             pair_copy(g, off).start()
-        for off in turns:
+            serve(beside, number, 2 * ny)
+        for number, off in enumerate(turns):
             own_part[lines] = product(p.chip(off))
+            serve(beside, ny + number, 2 * ny)
             pair_copy(g, off).wait_recv()
             both = own_part[lines] + pair_land[off, lines].astype(f32)
             both = both.reshape(count, capacity, width)
@@ -780,35 +783,39 @@
         for off in range(1, share):
             kv_relay(s, off).start()
 
-    for j in near[2:]:
+    half_near, some = len(near) // 2, len(second) // 2
+    for j in near[2 : half_near + 1]:
         arrive(j)
-    for j in near:
+    complete(0)
+    for j in near[half_near + 1 :]:
+        arrive(j)
+    for j in near[1:-1]:
         complete(j)
+    for j in second[:some]:
+        arrive(j)
+    complete(near[-1])
+    for j in second[some:]:
+        arrive(j)
     for j in near:
         settle(j)
     late[0].wait()
     late[1].wait()
-    open_up(0, [functools.partial(arrive, j) for j in second])
-    for j in second:
-        complete(j)
+    open_up(
+        0,
+        [(arrive, j) for j in third[:some]]
+        + [(complete, j) for j in second]
+        + [(arrive, j) for j in third[some:]],
+    )
     for j in second:
         settle(j)
-    open_up(1, [])
+    open_up(1, [(complete, j) for j in third])
     late[2].wait()
-    close_down(1)
-    for j in third:
-        arrive(j)
-    close_down(0)
-    for j in third:
-        complete(j)
-    for j in second:
-        finish(j)
+    close_down(1, [])
     for j in third:
         settle(j)
-    open_up(2, [functools.partial(kv_forward, n) for n in range(1, local_heads)])
-    close_down(2)
-    for j in near:
-        finish(j)
+    open_up(2, [(kv_forward, n) for n in range(1, local_heads)])
+    close_down(2, [(finish, j) for j in second])
+    close_down(0, [])
 
     late[3].wait()
     for j in range(n_ep):
@@ -861,6 +868,8 @@
             scores[b, at + part :] = block[part:]
             if b > 0:
                 running[at + part :] = jnp.maximum(running[at + part :], block[part:])
+    for j in third:
+        finish(j)
     row_max[...] = jnp.max(running[...], axis=1, keepdims=True)
     for b in range(n_ep):
         at = b * part
@@ -891,7 +900,7 @@
         head_copy(k).start()
     heads_all[p.t, p.e] = head_send[p.e]
 
-    for j in third:
+    for j in near:
         finish(j)
 
     gather = Spread(p, lambda t, s: heads_all.at[t, s], (hy0, hy1, hp0, hp1))

time: 61 us -> 54.9 us (0.900)
  Pallas kernels: 59.5 us -> 53.3 us
    pallas_call x1, Pallas kernels: 58.8 us -> 52.6 us  [fused_on_device(): pl.pallas_call(functools.partial(fused_kernel, n_ep, n_tp), out_shape=[ja...]
where the time goes in v1:
time: 54.9 us; the launch traced here: 54 us
  Pallas kernels  53.3 us (97%)
  between operations  0.64 us (1%)
    pallas_call x1, Pallas kernels, fused_on_device(): pl.pallas_call(functools.partial(fused_kernel, n_ep, n_tp), out_shape=[ja...  52.6 us

profile of v1, /device:TPU:0, one launch (start us, length us, event | category | flops | bytes accessed | tf_op | source)
XLA Modules:
  0.0 54.0 jit_solution(11576278596272138246)
XLA Ops:
  0.6 52.6 %fused.1 = (bf16[192,512]{1,0:T(8,128)(2,1)S(1)}, bf16[128,512]{1,0:T(8,128)(2,1)S(1)}) custom-call(bf16[192,2048]{1,0:T(8,128)(2,1)} %tokens_a.1, f32[1,2048]{1,0:T(1,128)} %bitcast.12, bf16[256,2048]{1,0:T(8,128)(2,1)} %w_q.1, bf16[256,2048]{1,0:T(8,128)(2,1)} %w_k.1, bf16[256,2048]{1,0:T(8,128)(2,1)} %w_v.1, bf16[4,2048]{1,0:T(4,128)(2,1)} %bitcast.11, ...), custom_call_target="tpu_custom_call" | custom-call | tf_op jit(solution)/shard_map/fused/pallas_call | solution.py:1021
  53.2 0.7 %deliver.1 = (bf16[192,512]{1,0:T(8,128)(2,1)}, bf16[128,512]{1,0:T(8,128)(2,1)}) custom-call(bf16[192,512]{1,0:T(8,128)(2,1)S(1)} %get-tuple-element.4.one, bf16[128,512]{1,0:T(8,128)(2,1)S(1)} %get-tuple-element.5.two), custom_call_target="tpu_custom_call" | custom-call | tf_op jit(solution)/shard_map/deliver/pallas_call | solution.py:1049

commit v2 on v1

--- a/solution.py
+++ b/solution.py
@@ -494,6 +494,41 @@
     return lax.broadcasted_iota(jnp.int32, shape, dim)
 
 
+class Relay:
+    def __init__(self, place, land, sems, batch):
+        self.p, self.land, self.batch = place, land, batch
+        self.ys, self.yr, self.ps, self.pr = sems
+
+    def y_copy(self, off, s, t, to):
+        block = self.land(t, s)
+        return remote(block, block, self.ys.at[0], self.yr.at[off - 1, s], self.p.e, to)
+
+    def p_copy(self, off, s, t):
+        block, p = self.land(t, s), self.p
+        return remote(block, block, self.ps.at[0], self.pr.at[self.batch(s)], p.e, p.partner)
+
+    def first(self, s):
+        p = self.p
+        for off in range(1, p.ny):
+            self.y_copy(off, s, p.t, p.chip(off)).start()
+        self.p_copy(0, s, p.t).start()
+
+    def relay(self, s):
+        p = self.p
+        for off in range(1, p.ny):
+            self.y_copy(off, s, p.chip(-off), p.chip(-off)).wait_recv()
+            self.p_copy(off, s, p.chip(-off)).start()
+
+    def settle(self, batch, blocks):
+        p = self.p
+        remote(blocks, blocks, self.ps.at[0], self.pr.at[batch], p.e, p.partner).wait_recv()
+
+    def sent(self, y_blocks, p_blocks):
+        p = self.p
+        remote(y_blocks, y_blocks, self.ys.at[0], self.yr.at[0, 0], p.e, p.partner).wait_send()
+        remote(p_blocks, p_blocks, self.ps.at[0], self.pr.at[0], p.e, p.partner).wait_send()
+
+
 def flipped(place, bits):
     at, weight = place, 1
     while bits:
@@ -527,9 +562,9 @@
     part = rows // share
     half = part // 2
     units = gate_held.shape[0]
-    near, quarter = range(n_ep // 2), n_ep // 4
-    third, second = range(n_ep // 2, 3 * quarter), range(3 * quarter, n_ep)
-    groups = [near, second, third]
+    quarter = n_ep // 4
+    near, second, third = range(2 * quarter), range(2 * quarter, 3 * quarter), range(3 * quarter, n_ep)
+    groups = [near[:quarter], range(quarter, 3 * quarter), third]
     own_share = p.e % share
     first = own_share * part
 
@@ -537,7 +572,7 @@
         return pl.ds(pl.multiple_of(t * width, width), width)
 
     def peer(j):
-        return flipped(p.e, j)
+        return flipped(p.e, j + quarter if j in second else j - quarter if j in third else j)
 
     barrier = pltpu.get_barrier_semaphore()
     for k in range(1, n_ep):
@@ -553,12 +588,7 @@
     )
 
     early = [(tokens_b, b_held), (routes, r_held), (gain_b, gb_held)]
-    middle = [(tokens_a, a_held), (gain_a, ga_held), (w_f, f_held), (b_f, bf_held)]
-    for h in range(local_heads):
-        mine_rows = pl.ds(h * HD, HD)
-        middle.append((w_k.at[mine_rows], kv_held.at[pl.ds(2 * h * HD, HD)]))
-        middle.append((w_v.at[mine_rows], kv_held.at[pl.ds((2 * h + 1) * HD, HD)]))
-    middle.append((w_q, q_held))
+    middle = [(tokens_a, a_held), (gain_a, ga_held), (w_f, f_held), (b_f, bf_held), (w_q, q_held)]
     late = [
         (w_gate, gate_held), (w_up, up_held), (w_down, down_held), (route_w, rw_held),
         (w_o, o_held),
@@ -570,8 +600,15 @@
             made.append(pltpu.make_async_copy(src, dst, lsem.at[number]))
             number += 1
         loads.append(made)
+    pieces = []
+    for h in range(local_heads):
+        mine_rows = pl.ds(h * HD, HD)
+        for at, src in ((2 * h, w_k), (2 * h + 1, w_v)):
+            there = kv_held.at[pl.ds(at * HD, HD)]
+            pieces.append(pltpu.make_async_copy(src.at[mine_rows], there, lsem.at[number]))
+    all_pieces = pltpu.make_async_copy(kv_held, kv_held, lsem.at[number])
     early, middle, late = loads
-    for load in early + middle:
+    for load in early + middle + pieces:
         load.start()
 
     for load in early:
@@ -583,6 +620,7 @@
     named_by = r_held[...]
     top_count = named_by.shape[0]
     place = lanes_of((n_ep, tokens), 0)
+    place = place + jnp.where(place < 2 * quarter, 0, jnp.where(place < 3 * quarter, 1, -1)) * quarter
     expert_at, weight = place, 1
     while weight < n_ep:
         flip = (p.e // weight) % 2
@@ -607,15 +645,20 @@
 
     def slot_copy(j):
         return remote(
-            slots.at[j], land.at[j, :, cols(p.t)], s0.at[j], s1.at[j], peer(j), p.t
-        )
-
-    spread = Spread(p, lambda t, j: land.at[j, :, cols(t)], (ys, yr, ps, pr))
+            slots.at[j], land.at[j, :, cols(p.t)], s0.at[0], s1.at[j], peer(j), p.t
+        )
+
+    spread = Relay(
+        p,
+        lambda t, j: land.at[j, :, cols(t)],
+        (ys, yr, ps, pr),
+        lambda j: [j in group for group in groups].index(True),
+    )
     for j in [*near[1:], *second, *third]:
         slot_copy(j).start()
     spread.first(0)
 
-    for load in middle:
+    for load in middle + [all_pieces]:
         load.wait()
     for load in late:
         load.start()
@@ -637,35 +680,33 @@
 
     def kv_copy(h):
         to = h * share + own_share
-        return remote(kv_send.at[h], kv_land.at[p.e], k0.at[h], k1.at[p.e], to, p.t)
+        return remote(kv_send.at[h], kv_land.at[p.e], k0.at[0], k1.at[p.e // share], to, p.t)
 
     def kv_arrival(n):
         s = (p.e // share + n) % local_heads * share + own_share
-        return remote(kv_send.at[0], kv_land.at[s], k0.at[0], k1.at[s], p.e, p.t), s
+        return remote(kv_send.at[0], kv_land.at[s], k0.at[0], k1.at[s // share], p.e, p.t), s
 
     def sibling(off):
         return p.e // share * share + (own_share + off) % share
 
     def kv_relay(s, off):
         return remote(
-            kv_land.at[s], kv_land.at[s], x0.at[off, s], x1.at[s], sibling(off), p.t
+            kv_land.at[s], kv_land.at[s], x0.at[0], x1.at[0], sibling(off), p.t
         )
 
     def q_copy(k):
         d = p.ep(k)
-        return remote(q_send.at[d], q_land.at[p.e], q0.at[d], q1.at[p.e], d, p.t)
-
-    def q_arrival(k):
-        s = p.ep(k)
-        return remote(q_send.at[s], q_land.at[s], q0.at[s], q1.at[s], s, p.t)
+        return remote(q_send.at[d], q_land.at[p.e], q0.at[0], q1.at[0], d, p.t)
 
     def g_copy(k):
         d = p.ep(k)
-        return remote(g_send.at[d // share], g_land.at[p.e], g0.at[d], g1.at[p.e], d, p.t)
-
-    def g_arrival(k):
-        s = p.ep(k)
-        return remote(g_send.at[0], g_land.at[s], g0.at[s], g1.at[s], s, p.t)
+        return remote(g_send.at[d // share], g_land.at[p.e], g0.at[0], g1.at[0], d, p.t)
+
+    def others(ref):
+        return ref.at[pl.ds(0, n_ep - 1)]
+
+    def batch_of(ref, send, recv):
+        return remote(ref, ref, send.at[0], recv.at[0], p.e, p.partner)
 
     key_value = by_rows(normed, kv_held[...]).astype(bf16)
     for h in range(local_heads):
@@ -702,11 +743,11 @@
     def complete(j):
         spread.relay(j)
 
-    def settle(j):
-        for off in range(ny):
-            spread.p_arrival(off, j).wait_recv()
-
-    cuts = [(at, min(at + 256, units)) for at in range(0, units, 256)]
+    def settle(g):
+        low_row, count = groups[g][0], len(groups[g])
+        spread.settle(g, land.at[pl.ds(low_row, count), :, pl.ds(0, ny * width)])
+
+    cuts = [(at, min(at + 512, units)) for at in range(0, units, 512)]
 
     def serve(beside, number, count):
         for act, *given in beside[len(beside) * number // count : len(beside) * (number + 1) // count]:
@@ -717,28 +758,28 @@
         block = land[low_row : low_row + count].reshape(count * capacity, features)
         lines = slice(low_row * capacity, (low_row + count) * capacity)
         for number, (low, high) in enumerate(cuts):
-            gated = by_rows(block, gate_held[low:high])
-            upped = by_rows(block, up_held[low:high])
-            hidden[lines, low:high] = (gated * lax.logistic(gated) * upped).astype(bf16)
+            gated = by_rows(gate_held[low:high], block)
+            upped = by_rows(up_held[low:high], block)
+            hidden[lines, low:high] = (gated * lax.logistic(gated) * upped).astype(bf16).T
             serve(beside, number, len(cuts))
 
     def pair_copy(g, off):
         low_row, count = groups[g][0], len(groups[g])
         lines = pl.ds(low_row * capacity, count * capacity)
         return remote(
-            pair_send.at[off, lines], pair_land.at[off, lines], p0.at[g, off], p1.at[g, off],
+            pair_send.at[off, lines], pair_land.at[off, lines], p0.at[0], p1.at[g, off],
             p.e, p.partner,
         )
 
     def y_copy(j, off, to):
         return remote(
             y_send.at[j, off - 1], y_land.at[j, off - 1],
-            z0.at[j, off - 1], z1.at[j, off - 1], p.e, p.chip(to),
+            z0.at[0], z1.at[j, off - 1], p.e, p.chip(to),
         )
 
     turns = [*range(1, ny), 0]
 
-    def close_down(g, beside):
+    def close_down(g, beside, held=()):
         low_row, count = groups[g][0], len(groups[g])
         lines = slice(low_row * capacity, (low_row + count) * capacity)
 
@@ -761,10 +802,11 @@
                     mine[j] = both[m]
                 else:
                     y_send[j, off - 1] = both[m].astype(bf16)
-                    y_copy(j, off, off).start()
+                    if j not in held:
+                        y_copy(j, off, off).start()
 
     def final_copy(j):
-        return remote(final.at[j], ret.at[j], a0.at[j], a1.at[j], peer(j), p.t)
+        return remote(final.at[j], ret.at[j], a0.at[0], a1.at[0], peer(j), p.t)
 
     def finish(j):
         total = mine[j]
@@ -783,39 +825,40 @@
         for off in range(1, share):
             kv_relay(s, off).start()
 
-    half_near, some = len(near) // 2, len(second) // 2
-    for j in near[2 : half_near + 1]:
+    some = len(third) // 2
+    for j in near[2 : quarter + 1]:
         arrive(j)
     complete(0)
-    for j in near[half_near + 1 :]:
+    for j in near[quarter + 1 :]:
         arrive(j)
     for j in near[1:-1]:
         complete(j)
-    for j in second[:some]:
+    for j in second:
         arrive(j)
-    complete(near[-1])
-    for j in second[some:]:
-        arrive(j)
-    for j in near:
-        settle(j)
+    settle(0)
     late[0].wait()
     late[1].wait()
-    open_up(
-        0,
-        [(arrive, j) for j in third[:some]]
-        + [(complete, j) for j in second]
-        + [(arrive, j) for j in third[some:]],
-    )
+    open_up(0, [])
+    complete(near[-1])
     for j in second:
-        settle(j)
-    open_up(1, [(complete, j) for j in third])
+        complete(j)
+    settle(1)
+    open_up(1, [(arrive, j) for j in third])
     late[2].wait()
-    close_down(1, [])
-    for j in third:
-        settle(j)
-    open_up(2, [(kv_forward, n) for n in range(1, local_heads)])
-    close_down(2, [(finish, j) for j in second])
-    close_down(0, [])
+    close_down(1, [], near)
+    for j in near[quarter:]:
+        for off in range(1, ny):
+            y_copy(j, off, off).start()
+    close_down(0, [(complete, j) for j in third], near)
+    for n in range(1, local_heads):
+        kv_forward(n)
+    settle(2)
+    open_up(2, [(finish, j) for j in second])
+    close_down(2, [])
+    behind = near[:quarter]
+    for j in behind:
+        for off in range(1, ny):
+            y_copy(j, off, off).start()
 
     late[3].wait()
     for j in range(n_ep):
@@ -829,13 +872,10 @@
         w_hi[j * capacity : (j + 1) * capacity] = high
         w_lo[j * capacity : (j + 1) * capacity] = (weight - high.astype(f32)).astype(bf16)
 
-    for k in range(1, n_ep):
-        g_arrival(k).wait_recv()
-        q_arrival(k).wait_recv()
-    for off in range(1, share):
-        for n in range(local_heads):
-            s = (p.e // share + n) % local_heads * share + (own_share + share - off) % share
-            remote(kv_send.at[0], kv_land.at[s], k0.at[0], x1.at[s], p.e, p.t).wait_recv()
+    batch_of(others(g_land), g0, g1).wait_recv()
+    batch_of(others(q_land), q0, q1).wait_recv()
+    relayed = kv_land.at[pl.ds(0, local_heads * (share - 1))]
+    batch_of(relayed, x0, x1).wait_recv()
     positions = lanes_of((part, rows), 1)
     asked = first + lanes_of((part, rows), 0)
     base = jnp.zeros((1, 1), f32)
@@ -868,8 +908,6 @@
             scores[b, at + part :] = block[part:]
             if b > 0:
                 running[at + part :] = jnp.maximum(running[at + part :], block[part:])
-    for j in third:
-        finish(j)
     row_max[...] = jnp.max(running[...], axis=1, keepdims=True)
     for b in range(n_ep):
         at = b * part
@@ -890,29 +928,34 @@
 
     def head_copy(k):
         d = peer(k)
-        return remote(head_send.at[d], heads_all.at[p.t, p.e], h0.at[d], h1.at[p.e], d, p.t)
+        return remote(head_send.at[d], heads_all.at[p.t, p.e], h0.at[0], h1.at[p.e], d, p.t)
 
     def head_arrival(k):
         s = peer(k)
-        return remote(head_send.at[s], heads_all.at[p.t, s], h0.at[s], h1.at[s], s, p.t)
+        return remote(head_send.at[s], heads_all.at[p.t, s], h0.at[0], h1.at[s], s, p.t)
 
     for k in range(1, n_ep):
         head_copy(k).start()
     heads_all[p.t, p.e] = head_send[p.e]
 
-    for j in near:
+    for j in near[quarter:]:
         finish(j)
-
-    gather = Spread(p, lambda t, s: heads_all.at[t, s], (hy0, hy1, hp0, hp1))
+    for j in third:
+        finish(j)
+
+    gather = Relay(p, lambda t, s: heads_all.at[t, s], (hy0, hy1, hp0, hp1), lambda s: 0)
     gather.first(p.e)
-    for k in range(1, n_ep):
+    for k in near[1:]:
+        head_arrival(k).wait_recv()
+        gather.first(peer(k))
+    for j in behind:
+        finish(j)
+    for k in [*second, *third]:
         head_arrival(k).wait_recv()
         gather.first(peer(k))
     for k in range(n_ep):
         gather.relay(peer(k))
-    for k in range(n_ep):
-        for off in range(ny):
-            gather.p_arrival(off, peer(k)).wait_recv()
+    gather.settle(0, heads_all.at[pl.ds(0, ny)])
     for t in range(n_tp):
         for pair in range(local_heads // 2):
             lanes = slice((t * local_heads + 2 * pair) * HD, (t * local_heads + 2 * pair + 2) * HD)
@@ -929,34 +972,24 @@
     late[4].wait()
     out_a[...] = jnp.dot(lhs[...], o_held[...], preferred_element_type=f32).astype(bf16)
 
-    for j in range(1, n_ep):
-        final_copy(j).wait_recv()
+    batch_of(others(ret), a0, a1).wait_recv()
     returned = ret[...].reshape(n_ep * capacity, width)
     over_slots = (((0,), (0,)), ((), ()))
     total = lax.dot_general(w_hi[...], returned, over_slots, preferred_element_type=f32)
     total = total + lax.dot_general(w_lo[...], returned, over_slots, preferred_element_type=f32)
     out_b[...] = total.astype(bf16)
 
-    for j in range(n_ep):
-        spread.wait_sent(j)
-        gather.wait_sent(peer(j))
-        for off in range(1, ny):
-            y_copy(j, off, off).wait_send()
-    for j in range(1, n_ep):
-        slot_copy(j).wait_send()
-        final_copy(j).wait_send()
-        q_copy(j).wait_send()
-        g_copy(j).wait_send()
-        head_copy(j).wait_send()
-    for n in range(1, local_heads):
-        kv_copy((p.e // share + n) % local_heads).wait_send()
-    for n in range(local_heads):
-        s = (p.e // share + n) % local_heads * share + own_share
-        for off in range(1, share):
-            kv_relay(s, off).wait_send()
-    for g in range(len(groups)):
-        for off in range(ny):
-            pair_copy(g, off).wait_send()
+    spread.sent(
+        land.at[:, :, pl.ds(0, (ny - 1) * width)], land.at[:, :, pl.ds(0, ny * width)]
+    )
+    gather.sent(heads_all.at[pl.ds(0, ny - 1)], heads_all.at[pl.ds(0, ny)])
+    for ref, send, recv in (
+        (others(slots), s0, s1), (others(q_send), q0, q1), (others(final), a0, a1),
+        (others(head_send), h0, h1), (pair_send, p0, a1), (y_send, z0, a1),
+        (others(g_land), g0, g1), (kv_send.at[pl.ds(0, local_heads - 1)], k0, k1),
+        (relayed, x0, x1),
+    ):
+        batch_of(ref, send, recv).wait_send()
 
 
 def fused_on_device(
@@ -1014,10 +1047,11 @@
         vmem((asked, 2 * HD), f32), vmem((n_ep, half, 2 * HD), bf16),
         vmem((n_tp, n_ep, half, 2 * HD), bf16), vmem((rows, n_tp * local_heads * HD), bf16),
     ]
-    sems = [DMA((13 + 2 * local_heads,)), DMA((n_ep,)), DMA((n_ep,))] + spread_sems(n_ep, n_tp)
-    sems += [DMA((local_heads,)), DMA((n_ep,)), DMA((share, n_ep)), DMA((n_ep,))]
-    sems += [DMA((n_ep,))] * 4 + [DMA((groups, ny))] * 2 + [DMA((n_ep, far))] * 2
-    sems += [DMA((n_ep,))] * 4 + spread_sems(n_ep, n_tp)
+    one = DMA((1,))
+    sems = [DMA((14,)), one, DMA((n_ep,)), one, DMA((far, n_ep)), one, DMA((groups,))]
+    sems += [one, DMA((local_heads,))] + [one] * 6
+    sems += [one, DMA((groups, ny)), one, DMA((n_ep, far)), one, one, one, DMA((n_ep,))]
+    sems += [one, DMA((far, n_ep)), one, one]
     return pl.pallas_call(
         functools.partial(fused_kernel, n_ep, n_tp),
         out_shape=[
@@ -1065,7 +1099,7 @@
     rows, local_heads = arguments[0].shape[0], arguments[5].shape[1]
     share = n_ep // local_heads
     packed = local_heads % 2 == 0 and n_ep % local_heads == 0
-    packed = packed and n_ep >= 8 and n_ep & (n_ep - 1) == 0
+    packed = packed and n_ep >= 8 and n_ep & (n_ep - 1) == 0 and lax.axis_size("tp") >= 4
     if packed and rows % (32 * share) == 0:
         return tuple(deliver(*fused_on_device(*arguments)))
     return on_device(*arguments)

time: 54.9 us -> 51 us (0.929); the launches traced: 54 us -> 50.8 us
  Pallas kernels: 53.3 us -> 50.2 us
    pallas_call x1, Pallas kernels: 52.6 us -> 49.4 us  [fused_on_device(): pl.pallas_call(functools.partial(fused_kernel, n_ep, n_tp), out_shape=[ja...]
where the time goes in v2:
time: 51 us; the launch traced here: 50.8 us
  Pallas kernels  50.2 us (98%)
  between operations  0.64 us (1%)
    pallas_call x1, Pallas kernels, fused_on_device(): pl.pallas_call(functools.partial(fused_kernel, n_ep, n_tp), out_shape=[ja...  49.4 us

profile of v2, /device:TPU:0, one launch (start us, length us, event | category | flops | bytes accessed | tf_op | source)
XLA Modules:
  0.0 50.8 jit_solution(8888156338385118459)
XLA Ops:
  0.6 49.4 %fused.1 = (bf16[192,512]{1,0:T(8,128)(2,1)S(1)}, bf16[128,512]{1,0:T(8,128)(2,1)S(1)}) custom-call(bf16[192,2048]{1,0:T(8,128)(2,1)} %tokens_a.1, f32[1,2048]{1,0:T(1,128)} %bitcast.12, bf16[256,2048]{1,0:T(8,128)(2,1)} %w_q.1, bf16[256,2048]{1,0:T(8,128)(2,1)} %w_k.1, bf16[256,2048]{1,0:T(8,128)(2,1)} %w_v.1, bf16[4,2048]{1,0:T(4,128)(2,1)} %bitcast.11, ...), custom_call_target="tpu_custom_call" | custom-call | tf_op jit(solution)/shard_map/fused/pallas_call | solution.py:1055
  50.1 0.7 %deliver.1 = (bf16[192,512]{1,0:T(8,128)(2,1)}, bf16[128,512]{1,0:T(8,128)(2,1)}) custom-call(bf16[192,512]{1,0:T(8,128)(2,1)S(1)} %get-tuple-element.4.one, bf16[128,512]{1,0:T(8,128)(2,1)S(1)} %get-tuple-element.5.two), custom_call_target="tpu_custom_call" | custom-call | tf_op jit(solution)/shard_map/deliver/pallas_call | solution.py:1083

commit v3 on v2

--- a/solution.py
+++ b/solution.py
@@ -545,10 +545,10 @@
     out_a, out_b,
     a_held, ga_held, q_held, kv_held, f_held, bf_held, o_held, b_held, gb_held, r_held, rw_held,
     gate_held, up_held, down_held,
-    slots, land, w_hi, w_lo, kv_send, q_send, g_send, kv_land, q_land, g_land,
+    slots, slots_more, land, w_hi, w_lo, kv_send, q_send, g_send, kv_land, q_land, g_land,
     hidden, pair_send, pair_land, own_part, mine, y_send, y_land, final, ret,
-    q_all, q_cum, scores, running, row_max, attended, head_send, heads_all, lhs,
-    lsem, s0, s1, ys, yr, ps, pr, k0, k1, x0, x1, q0, q1, g0, g1,
+    q_all, q_cum, scores, running, row_max, attended, head_send, heads_all, lhs, mixed,
+    lsem, s0, s1, m0, m1, ys, yr, ps, pr, k0, k1, x0, x1, q0, q1, g0, g1,
     p0, p1, z0, z1, a0, a1, h0, h1, hy0, hy1, hp0, hp1,
 ):
     p = Place(n_ep, n_tp)
@@ -616,7 +616,7 @@
     values = b_held[...].astype(f32)
     square = jnp.mean(values * values, axis=-1, keepdims=True)
     scale = lax.rsqrt(jnp.maximum(square, MEAN_FLOOR))
-    own_columns = (b_held[:, cols(p.t)].astype(f32) * scale * gb_held[:, cols(p.t)]).astype(bf16)
+    b_held[...] = (values * scale * gb_held[...]).astype(bf16)
     named_by = r_held[...]
     top_count = named_by.shape[0]
     place = lanes_of((n_ep, tokens), 0)
@@ -633,20 +633,34 @@
     ranks = jnp.where(named > 0, ranks, -1.0).astype(jnp.int32)
     slot_at = lanes_of((capacity, tokens), 0)
     picks = [ranks[j : j + 1, :] == slot_at for j in range(n_ep)]
-    for j in range(n_ep):
-        block = jnp.dot(
-            picks[j].astype(f32).astype(bf16), own_columns, preferred_element_type=f32
-        ).astype(bf16)
-        if j == 0:
-            land[0, :, cols(p.t)] = block
-        else:
-            slots[j] = block
+    picks = [pick.astype(f32).astype(bf16) for pick in picks]
+
+    def picked(j, lanes):
+        return jnp.dot(picks[j], b_held[:, lanes], preferred_element_type=f32).astype(bf16)
+
+    for j in range(1, n_ep):
+        slots[j] = picked(j, cols(p.t))
+    for j in near[1:]:
+        for off in range(1, ny):
+            slots_more[j, off - 1] = picked(j, cols(p.chip(-off)))
     pl.semaphore_wait(barrier, n_ep - 1 + ny - 1 + 1)
 
     def slot_copy(j):
         return remote(
             slots.at[j], land.at[j, :, cols(p.t)], s0.at[0], s1.at[j], peer(j), p.t
         )
+
+    def more_copy(j, off):
+        return remote(
+            slots_more.at[j, off - 1], land.at[j, :, cols(p.chip(-off))],
+            m0.at[0], m1.at[j, off - 1], peer(j), p.t,
+        )
+
+    def send(j):
+        slot_copy(j).start()
+        if j in near:
+            for off in range(1, ny):
+                more_copy(j, off).start()
 
     spread = Relay(
         p,
@@ -654,9 +668,9 @@
         (ys, yr, ps, pr),
         lambda j: [j in group for group in groups].index(True),
     )
-    for j in [*near[1:], *second, *third]:
-        slot_copy(j).start()
-    spread.first(0)
+    for j in [*near[1:quarter], *second, *near[quarter:], *third]:
+        send(j)
+    land[0] = picked(0, slice(None))
 
     for load in middle + [all_pieces]:
         load.wait()
@@ -717,8 +731,6 @@
     kv_land[p.e] = kv_send[own_head]
     for off in range(1, share):
         kv_relay(p.e, off).start()
-    slot_copy(1).wait_recv()
-    spread.first(1)
     queries = by_rows(normed, q_held[...]) * HD ** (-0.5)
     left = lanes_of((half, 2 * HD), 1) < HD
     for pair in range(local_heads // 2):
@@ -738,14 +750,20 @@
 
     def arrive(j):
         slot_copy(j).wait_recv()
-        spread.first(j)
+        if j in near:
+            spread.p_copy(0, j, p.t).start()
+            for off in range(1, ny):
+                more_copy(j, off).wait_recv()
+                spread.p_copy(off, j, p.chip(-off)).start()
+        else:
+            spread.first(j)
 
     def complete(j):
         spread.relay(j)
 
     def settle(g):
-        low_row, count = groups[g][0], len(groups[g])
-        spread.settle(g, land.at[pl.ds(low_row, count), :, pl.ds(0, ny * width)])
+        count = len(groups[g]) - (0 in groups[g])
+        spread.settle(g, land.at[pl.ds(0, count), :, pl.ds(0, ny * width)])
 
     cuts = [(at, min(at + 512, units)) for at in range(0, units, 512)]
 
@@ -825,33 +843,30 @@
         for off in range(1, share):
             kv_relay(s, off).start()
 
-    some = len(third) // 2
-    for j in near[2 : quarter + 1]:
-        arrive(j)
-    complete(0)
-    for j in near[quarter + 1 :]:
-        arrive(j)
-    for j in near[1:-1]:
-        complete(j)
-    for j in second:
+    some = len(second) // 2
+    for j in [*near[1:quarter], *second[:some]]:
         arrive(j)
     settle(0)
     late[0].wait()
     late[1].wait()
-    open_up(0, [])
-    complete(near[-1])
-    for j in second:
-        complete(j)
+    open_up(0, [(arrive, j) for j in [*second[some:], *near[quarter : quarter + quarter // 2]]])
+    late[2].wait()
+    close_down(
+        0,
+        [(arrive, j) for j in near[quarter + quarter // 2 :]] + [(complete, j) for j in second],
+        near,
+    )
     settle(1)
     open_up(1, [(arrive, j) for j in third])
-    late[2].wait()
     close_down(1, [], near)
     for j in near[quarter:]:
         for off in range(1, ny):
             y_copy(j, off, off).start()
-    close_down(0, [(complete, j) for j in third], near)
+    complete(third[0])
     for n in range(1, local_heads):
         kv_forward(n)
+    for j in third[1:]:
+        complete(j)
     settle(2)
     open_up(2, [(finish, j) for j in second])
     close_down(2, [])
@@ -934,7 +949,7 @@
         s = peer(k)
         return remote(head_send.at[s], heads_all.at[p.t, s], h0.at[0], h1.at[s], s, p.t)
 
-    for k in range(1, n_ep):
+    for k in [*second, *third, *near[1:]]:
         head_copy(k).start()
     heads_all[p.t, p.e] = head_send[p.e]
 
@@ -955,10 +970,11 @@
         gather.first(peer(k))
     for k in range(n_ep):
         gather.relay(peer(k))
-    gather.settle(0, heads_all.at[pl.ds(0, ny)])
-    for t in range(n_tp):
+    late[4].wait()
+
+    def project(t):
         for pair in range(local_heads // 2):
-            lanes = slice((t * local_heads + 2 * pair) * HD, (t * local_heads + 2 * pair + 2) * HD)
+            lanes = slice(2 * pair * HD, 2 * (pair + 1) * HD)
             for x in range(share):
                 one = heads_all[t, 2 * pair * share + x].astype(f32)
                 two = heads_all[t, (2 * pair + 1) * share + x].astype(f32)
@@ -969,8 +985,18 @@
                 lhs[at + half : at + part, lanes] = jnp.where(
                     left, pltpu.roll(one, HD, 1), two
                 ).astype(bf16)
-    late[4].wait()
-    out_a[...] = jnp.dot(lhs[...], o_held[...], preferred_element_type=f32).astype(bf16)
+        deep = local_heads * HD
+        here = o_held[pl.ds(pl.multiple_of(t * deep, deep), deep), :]
+        return jnp.dot(lhs[...], here, preferred_element_type=f32)
+
+    mixed[...] = project(p.t)
+    for off in range(1, ny):
+        mixed[...] = mixed[...] + project(p.chip(-off))
+    gather.settle(0, heads_all.at[pl.ds(0, ny)])
+    for off in range(ny - 1):
+        mixed[...] = mixed[...] + project(p.y_at(-off) * 2 + (1 - p.c))
+    last_part = project(p.y_at(-(ny - 1)) * 2 + (1 - p.c))
+    out_a[...] = (mixed[...] + last_part).astype(bf16)
 
     batch_of(others(ret), a0, a1).wait_recv()
     returned = ret[...].reshape(n_ep * capacity, width)
@@ -980,11 +1006,12 @@
     out_b[...] = total.astype(bf16)
 
     spread.sent(
-        land.at[:, :, pl.ds(0, (ny - 1) * width)], land.at[:, :, pl.ds(0, ny * width)]
+        land.at[pl.ds(0, n_ep - len(near)), :, pl.ds(0, (ny - 1) * width)],
+        land.at[pl.ds(0, n_ep - 1), :, pl.ds(0, ny * width)],
     )
     gather.sent(heads_all.at[pl.ds(0, ny - 1)], heads_all.at[pl.ds(0, ny)])
     for ref, send, recv in (
-        (others(slots), s0, s1), (others(q_send), q0, q1), (others(final), a0, a1),
+        (others(slots), s0, s1), (slots_more.at[pl.ds(0, len(near) - 1)], m0, s1), (others(q_send), q0, q1), (others(final), a0, a1),
         (others(head_send), h0, h1), (pair_send, p0, a1), (y_send, z0, a1),
         (others(g_land), g0, g1), (kv_send.at[pl.ds(0, local_heads - 1)], k0, k1),
         (relayed, x0, x1),
@@ -1029,7 +1056,8 @@
         vmem((top_count, tokens), f32),
         vmem((units, features), bf16), vmem((units, features), bf16),
         vmem((units, features), bf16),
-        vmem((n_ep, capacity, width), bf16), vmem((n_ep, capacity, features), bf16),
+        vmem((n_ep, capacity, width), bf16), vmem((n_ep // 2, far, capacity, width), bf16),
+        vmem((n_ep, capacity, features), bf16),
         vmem((n_ep * capacity, tokens), bf16), vmem((n_ep * capacity, tokens), bf16),
         vmem((local_heads, rows, 2 * HD), bf16), vmem((n_ep, half, 2 * HD), bf16),
         vmem((local_heads, 1, rows), f32),
@@ -1045,10 +1073,10 @@
         vmem((asked, 2 * HD), bf16), vmem((asked, 1), f32),
         vmem((n_ep, asked, rows), f32), vmem((asked, rows), f32), vmem((asked, 1), f32),
         vmem((asked, 2 * HD), f32), vmem((n_ep, half, 2 * HD), bf16),
-        vmem((n_tp, n_ep, half, 2 * HD), bf16), vmem((rows, n_tp * local_heads * HD), bf16),
+        vmem((n_tp, n_ep, half, 2 * HD), bf16), vmem((rows, local_heads * HD), bf16), vmem((rows, width), f32),
     ]
     one = DMA((1,))
-    sems = [DMA((14,)), one, DMA((n_ep,)), one, DMA((far, n_ep)), one, DMA((groups,))]
+    sems = [DMA((14,)), one, DMA((n_ep,)), one, DMA((n_ep // 2, far)), one, DMA((far, n_ep)), one, DMA((groups,))]
     sems += [one, DMA((local_heads,))] + [one] * 6
     sems += [one, DMA((groups, ny)), one, DMA((n_ep, far)), one, one, one, DMA((n_ep,))]
     sems += [one, DMA((far, n_ep)), one, one]

time: 51 us -> 48.2 us (0.945)
  Pallas kernels: 50.2 us -> 47 us
    pallas_call x1, Pallas kernels: 49.4 us -> 46.2 us  [fused_on_device(): pl.pallas_call(functools.partial(fused_kernel, n_ep, n_tp), out_shape=[ja...]
where the time goes in v3:
time: 48.2 us; the launch traced here: 47.6 us
  Pallas kernels  47 us (98%)
  between operations  0.64 us (1%)
    pallas_call x1, Pallas kernels, fused_on_device(): pl.pallas_call(functools.partial(fused_kernel, n_ep, n_tp), out_shape=[ja...  46.2 us

profile of v3, /device:TPU:0, one launch (start us, length us, event | category | flops | bytes accessed | tf_op | source)
XLA Modules:
  0.0 47.6 jit_solution(3542968726757003131)
XLA Ops:
  0.6 46.2 %fused.1 = (bf16[192,512]{1,0:T(8,128)(2,1)S(1)}, bf16[128,512]{1,0:T(8,128)(2,1)S(1)}) custom-call(bf16[192,2048]{1,0:T(8,128)(2,1)} %tokens_a.1, f32[1,2048]{1,0:T(1,128)} %bitcast.12, bf16[256,2048]{1,0:T(8,128)(2,1)} %w_q.1, bf16[256,2048]{1,0:T(8,128)(2,1)} %w_k.1, bf16[256,2048]{1,0:T(8,128)(2,1)} %w_v.1, bf16[4,2048]{1,0:T(4,128)(2,1)} %bitcast.11, ...), custom_call_target="tpu_custom_call" | custom-call | tf_op jit(solution)/shard_map/fused/pallas_call | solution.py:1083
  46.9 0.7 %deliver.1 = (bf16[192,512]{1,0:T(8,128)(2,1)}, bf16[128,512]{1,0:T(8,128)(2,1)}) custom-call(bf16[192,512]{1,0:T(8,128)(2,1)S(1)} %get-tuple-element.4.one, bf16[128,512]{1,0:T(8,128)(2,1)S(1)} %get-tuple-element.5.two), custom_call_target="tpu_custom_call" | custom-call | tf_op jit(solution)/shard_map/deliver/pallas_call | solution.py:1111

commit v4 on v3

--- a/solution.py
+++ b/solution.py
@@ -562,9 +562,16 @@
     part = rows // share
     half = part // 2
     units = gate_held.shape[0]
-    quarter = n_ep // 4
-    near, second, third = range(2 * quarter), range(2 * quarter, 3 * quarter), range(3 * quarter, n_ep)
-    groups = [near[:quarter], range(quarter, 3 * quarter), third]
+    eighth = n_ep // 8
+    order = [0, 1, 2, 6, 7, 3, 4, 5]
+
+    def places(*eighths):
+        return [order.index(k) * eighth + i for k in eighths for i in range(eighth)]
+
+    own, second, third = places(0), places(6, 7), places(4, 5)
+    near = [*own[1:], *places(1, 2, 3)]
+    groups = [range(eighth), range(eighth, 5 * eighth), range(5 * eighth, n_ep)]
+    early_near, late_near = places(1, 2), places(3)
     own_share = p.e % share
     first = own_share * part
 
@@ -572,7 +579,7 @@
         return pl.ds(pl.multiple_of(t * width, width), width)
 
     def peer(j):
-        return flipped(p.e, j + quarter if j in second else j - quarter if j in third else j)
+        return flipped(p.e, order[j // eighth] * eighth + j % eighth)
 
     barrier = pltpu.get_barrier_semaphore()
     for k in range(1, n_ep):
@@ -620,7 +627,8 @@
     named_by = r_held[...]
     top_count = named_by.shape[0]
     place = lanes_of((n_ep, tokens), 0)
-    place = place + jnp.where(place < 2 * quarter, 0, jnp.where(place < 3 * quarter, 1, -1)) * quarter
+    moved = [jnp.where(place // eighth == k, order[k] - k, 0) for k in range(8)]
+    place = place + sum(moved[1:], moved[0]) * eighth
     expert_at, weight = place, 1
     while weight < n_ep:
         flip = (p.e // weight) % 2
@@ -640,9 +648,9 @@
 
     for j in range(1, n_ep):
         slots[j] = picked(j, cols(p.t))
-    for j in near[1:]:
+    for j in near:
         for off in range(1, ny):
-            slots_more[j, off - 1] = picked(j, cols(p.chip(-off)))
+            slots_more[near.index(j), off - 1] = picked(j, cols(p.chip(-off)))
     pl.semaphore_wait(barrier, n_ep - 1 + ny - 1 + 1)
 
     def slot_copy(j):
@@ -652,8 +660,8 @@
 
     def more_copy(j, off):
         return remote(
-            slots_more.at[j, off - 1], land.at[j, :, cols(p.chip(-off))],
-            m0.at[0], m1.at[j, off - 1], peer(j), p.t,
+            slots_more.at[near.index(j), off - 1], land.at[j, :, cols(p.chip(-off))],
+            m0.at[0], m1.at[near.index(j), off - 1], peer(j), p.t,
         )
 
     def send(j):
@@ -668,7 +676,7 @@
         (ys, yr, ps, pr),
         lambda j: [j in group for group in groups].index(True),
     )
-    for j in [*near[1:quarter], *second, *near[quarter:], *third]:
+    for j in [*own[1:], *places(1), *second, *places(2, 3), *third]:
         send(j)
     land[0] = picked(0, slice(None))
 
@@ -843,23 +851,23 @@
         for off in range(1, share):
             kv_relay(s, off).start()
 
-    some = len(second) // 2
-    for j in [*near[1:quarter], *second[:some]]:
+    for j in own[1:]:
         arrive(j)
-    settle(0)
+    if own[1:]:
+        settle(0)
     late[0].wait()
     late[1].wait()
-    open_up(0, [(arrive, j) for j in [*second[some:], *near[quarter : quarter + quarter // 2]]])
+    open_up(0, [(arrive, j) for j in places(1)])
     late[2].wait()
-    close_down(
-        0,
-        [(arrive, j) for j in near[quarter + quarter // 2 :]] + [(complete, j) for j in second],
-        near,
-    )
+    close_down(0, [(arrive, j) for j in second], own)
+    for j in places(2):
+        arrive(j)
+    for j in second:
+        complete(j)
     settle(1)
-    open_up(1, [(arrive, j) for j in third])
+    open_up(1, [(arrive, j) for j in [*third, *late_near]])
     close_down(1, [], near)
-    for j in near[quarter:]:
+    for j in early_near:
         for off in range(1, ny):
             y_copy(j, off, off).start()
     complete(third[0])
@@ -869,8 +877,8 @@
         complete(j)
     settle(2)
     open_up(2, [(finish, j) for j in second])
-    close_down(2, [])
-    behind = near[:quarter]
+    close_down(2, [], near)
+    behind = [*late_near, *own]
     for j in behind:
         for off in range(1, ny):
             y_copy(j, off, off).start()
@@ -949,18 +957,18 @@
         s = peer(k)
         return remote(head_send.at[s], heads_all.at[p.t, s], h0.at[0], h1.at[s], s, p.t)
 
-    for k in [*second, *third, *near[1:]]:
+    for k in [*second, *third, *near]:
         head_copy(k).start()
     heads_all[p.t, p.e] = head_send[p.e]
 
-    for j in near[quarter:]:
+    for j in early_near:
         finish(j)
     for j in third:
         finish(j)
 
     gather = Relay(p, lambda t, s: heads_all.at[t, s], (hy0, hy1, hp0, hp1), lambda s: 0)
     gather.first(p.e)
-    for k in near[1:]:
+    for k in near:
         head_arrival(k).wait_recv()
         gather.first(peer(k))
     for j in behind:
@@ -1006,12 +1014,12 @@
     out_b[...] = total.astype(bf16)
 
     spread.sent(
-        land.at[pl.ds(0, n_ep - len(near)), :, pl.ds(0, (ny - 1) * width)],
+        land.at[pl.ds(0, len(second) + len(third)), :, pl.ds(0, (ny - 1) * width)],
         land.at[pl.ds(0, n_ep - 1), :, pl.ds(0, ny * width)],
     )
     gather.sent(heads_all.at[pl.ds(0, ny - 1)], heads_all.at[pl.ds(0, ny)])
     for ref, send, recv in (
-        (others(slots), s0, s1), (slots_more.at[pl.ds(0, len(near) - 1)], m0, s1), (others(q_send), q0, q1), (others(final), a0, a1),
+        (others(slots), s0, s1), (slots_more, m0, s1), (others(q_send), q0, q1), (others(final), a0, a1),
         (others(head_send), h0, h1), (pair_send, p0, a1), (y_send, z0, a1),
         (others(g_land), g0, g1), (kv_send.at[pl.ds(0, local_heads - 1)], k0, k1),
         (relayed, x0, x1),
@@ -1056,7 +1064,7 @@
         vmem((top_count, tokens), f32),
         vmem((units, features), bf16), vmem((units, features), bf16),
         vmem((units, features), bf16),
-        vmem((n_ep, capacity, width), bf16), vmem((n_ep // 2, far, capacity, width), bf16),
+        vmem((n_ep, capacity, width), bf16), vmem((n_ep // 2 - 1, far, capacity, width), bf16),
         vmem((n_ep, capacity, features), bf16),
         vmem((n_ep * capacity, tokens), bf16), vmem((n_ep * capacity, tokens), bf16),
         vmem((local_heads, rows, 2 * HD), bf16), vmem((n_ep, half, 2 * HD), bf16),
@@ -1076,7 +1084,7 @@
         vmem((n_tp, n_ep, half, 2 * HD), bf16), vmem((rows, local_heads * HD), bf16), vmem((rows, width), f32),
     ]
     one = DMA((1,))
-    sems = [DMA((14,)), one, DMA((n_ep,)), one, DMA((n_ep // 2, far)), one, DMA((far, n_ep)), one, DMA((groups,))]
+    sems = [DMA((14,)), one, DMA((n_ep,)), one, DMA((n_ep // 2 - 1, far)), one, DMA((far, n_ep)), one, DMA((groups,))]
     sems += [one, DMA((local_heads,))] + [one] * 6
     sems += [one, DMA((groups, ny)), one, DMA((n_ep, far)), one, one, one, DMA((n_ep,))]
     sems += [one, DMA((far, n_ep)), one, one]

time: 48.2 us -> 46.2 us (0.959)
  Pallas kernels: 47 us -> 45.4 us
    pallas_call x1, Pallas kernels: 46.2 us -> 44.7 us  [fused_on_device(): pl.pallas_call(functools.partial(fused_kernel, n_ep, n_tp), out_shape=[ja...]
where the time goes in v4:
time: 46.2 us; the launch traced here: 46.1 us
  Pallas kernels  45.4 us (98%)
  between operations  0.64 us (1%)
    pallas_call x1, Pallas kernels, fused_on_device(): pl.pallas_call(functools.partial(fused_kernel, n_ep, n_tp), out_shape=[ja...  44.7 us

profile of v4, /device:TPU:0, one launch (start us, length us, event | category | flops | bytes accessed | tf_op | source)
XLA Modules:
  0.0 46.1 jit_solution(1920699461320888176)
XLA Ops:
  0.6 44.7 %fused.1 = (bf16[192,512]{1,0:T(8,128)(2,1)S(1)}, bf16[128,512]{1,0:T(8,128)(2,1)S(1)}) custom-call(bf16[192,2048]{1,0:T(8,128)(2,1)} %tokens_a.1, f32[1,2048]{1,0:T(1,128)} %bitcast.12, bf16[256,2048]{1,0:T(8,128)(2,1)} %w_q.1, bf16[256,2048]{1,0:T(8,128)(2,1)} %w_k.1, bf16[256,2048]{1,0:T(8,128)(2,1)} %w_v.1, bf16[4,2048]{1,0:T(4,128)(2,1)} %bitcast.11, ...), custom_call_target="tpu_custom_call" | custom-call | tf_op jit(solution)/shard_map/fused/pallas_call | solution.py:1091
  45.3 0.7 %deliver.1 = (bf16[192,512]{1,0:T(8,128)(2,1)}, bf16[128,512]{1,0:T(8,128)(2,1)}) custom-call(bf16[192,512]{1,0:T(8,128)(2,1)S(1)} %get-tuple-element.4.one, bf16[128,512]{1,0:T(8,128)(2,1)S(1)} %get-tuple-element.5.two), custom_call_target="tpu_custom_call" | custom-call | tf_op jit(solution)/shard_map/deliver/pallas_call | solution.py:1119

commit v5 on v4

--- a/solution.py
+++ b/solution.py
@@ -878,10 +878,6 @@
     settle(2)
     open_up(2, [(finish, j) for j in second])
     close_down(2, [], near)
-    behind = [*late_near, *own]
-    for j in behind:
-        for off in range(1, ny):
-            y_copy(j, off, off).start()
 
     late[3].wait()
     for j in range(n_ep):
@@ -940,6 +936,10 @@
             attended[...] = product
         else:
             attended[at:] = attended[at:] + product
+    behind = [*late_near, *own]
+    for j in behind:
+        for off in range(1, ny):
+            y_copy(j, off, off).start()
     right = lanes_of((part, 2 * HD), 1) >= HD
     for b in range(n_ep):
         block = jnp.where(right, attended[b * part : (b + 1) * part], 0.0)

time: 46.2 us -> 46.2 us (level)
  no operation moved by 1% of the time
where the time goes in v5:
time: 46.2 us; the launch traced here: 46.1 us
  Pallas kernels  45.4 us (98%)
  between operations  0.64 us (1%)
    pallas_call x1, Pallas kernels, fused_on_device(): pl.pallas_call(functools.partial(fused_kernel, n_ep, n_tp), out_shape=[ja...  44.7 us

profile of v5, /device:TPU:0, one launch (start us, length us, event | category | flops | bytes accessed | tf_op | source)
XLA Modules:
  0.0 46.1 jit_solution(17565876556719268641)
XLA Ops:
  0.6 44.7 %fused.1 = (bf16[192,512]{1,0:T(8,128)(2,1)S(1)}, bf16[128,512]{1,0:T(8,128)(2,1)S(1)}) custom-call(bf16[192,2048]{1,0:T(8,128)(2,1)} %tokens_a.1, f32[1,2048]{1,0:T(1,128)} %bitcast.12, bf16[256,2048]{1,0:T(8,128)(2,1)} %w_q.1, bf16[256,2048]{1,0:T(8,128)(2,1)} %w_k.1, bf16[256,2048]{1,0:T(8,128)(2,1)} %w_v.1, bf16[4,2048]{1,0:T(4,128)(2,1)} %bitcast.11, ...), custom_call_target="tpu_custom_call" | custom-call | tf_op jit(solution)/shard_map/fused/pallas_call | solution.py:1091
  45.3 0.7 %deliver.1 = (bf16[192,512]{1,0:T(8,128)(2,1)}, bf16[128,512]{1,0:T(8,128)(2,1)}) custom-call(bf16[192,512]{1,0:T(8,128)(2,1)S(1)} %get-tuple-element.4.one, bf16[128,512]{1,0:T(8,128)(2,1)S(1)} %get-tuple-element.5.two), custom_call_target="tpu_custom_call" | custom-call | tf_op jit(solution)/shard_map/deliver/pallas_call | solution.py:1119
